TPU v7x, 32 devices: a whole 2x2x4 slice. The times are simulated.
32 devices in a mesh: sp: 4 (over z), tp: 8 (over y, x, core).
Axes of the slice: x: 2, y: 2, z: 4, core: 2. Of those that a mesh axis runs over, the one named last changes fastest.
Arguments:
- token_values: bfloat16 [1024, 2048], P('sp', 'tp'), may hold values from -6 to 6
- write_keys: bfloat16 [1024, 1024], P('sp', 'tp'), may hold values from -0.4375 to 0.4375
- read_keys: bfloat16 [1024, 1024], P('sp', 'tp'), may hold values from -0.4375 to 0.4375
- log_decay: float32 [32, 1024], P('tp', 'sp'), may hold values from -0.7 to 0, as said below
- out_gate: bfloat16 [1024, 2048], P('sp', 'tp'), may hold values from -6 to 6
- out_proj: bfloat16 [4096, 2048], P(None, 'tp'), may hold values from -0.125 to 0.125
- mixed: bfloat16 [1024, 4096], P('sp'), may hold values from -6 to 6
- cotangent: bfloat16 [1024, 4096], P('sp'), may hold values from -8 to 8
- route_ids: int32 [1024, 2], P('sp'), may hold values from 0 to 3, all different within a row; in each aligned block of 256 rows (0 to 255, 256 to 511, ...) at most 192 rows name the same one
- route_weights: float32 [1024, 2], P('sp'), may hold values from 0.25 to 1
- w_gate: bfloat16 [4, 4096, 2048], P('sp', None, 'tp'), may hold values from -0.09375 to 0.09375
- w_up: bfloat16 [4, 4096, 2048], P('sp', None, 'tp'), may hold values from -0.09375 to 0.09375
- w_down: bfloat16 [4, 2048, 4096], P('sp', 'tp'), may hold values from -0.125 to 0.125
Outputs:
- value_grad: bfloat16 [1024, 2048], P('sp', 'tp')
- write_grad: bfloat16 [1024, 1024], P('sp', 'tp')
- read_grad: bfloat16 [1024, 1024], P('sp', 'tp')
- gate_grad: bfloat16 [1024, 2048], P('sp', 'tp')
- proj_grad: float32 [4096, 2048], P('sp', 'tp')
- gate_weight_grad: bfloat16 [4, 4096, 2048], P('sp', None, 'tp')
- up_weight_grad: bfloat16 [4, 4096, 2048], P('sp', None, 'tp')
- down_weight_grad: bfloat16 [4, 2048, 4096], P('sp', 'tp')
Inputs may be any that keep to these rules, and one draw needn't show every extreme that they name: `route_ids`: each row names 2 different experts. Within the rows of one device no expert is named more than 192 times, and in every draw some expert is named exactly 192 times by the rows of some device. `log_decay`: every entry is negative.
All inputs are finite; a program needn't handle non-finite values.
Results may differ from a plain program's by a relative error of at most 0.019.
Values may be sent and summed in bfloat16 or wider, within the bound.
A program may use at most 128 MiB of HBM per device.

v0:
```python
import jax
import jax.numpy as jnp
from jax import lax
from jax.sharding import PartitionSpec as P

HEAD_DIM = 64
STATE = 128
BLOCK = 64


highest = lax.Precision.HIGHEST


def mix_blocks(token_values, write_keys, read_keys, log_decay, entering):
    length = token_values.shape[0]
    heads = log_decay.shape[0]
    groups = write_keys.shape[1] // STATE
    per_group = heads // groups
    blocks = length // BLOCK
    inputs = token_values.reshape(blocks, BLOCK, groups, per_group, HEAD_DIM)
    writes = write_keys.reshape(blocks, BLOCK, groups, STATE)
    reads = read_keys.reshape(blocks, BLOCK, groups, STATE)
    decay = log_decay.reshape(groups, per_group, blocks, BLOCK).transpose(2, 3, 0, 1)
    cumul = jnp.cumsum(decay, axis=1)
    spans = cumul[:, :, None] - cumul[:, None, :]
    position = jnp.arange(BLOCK, dtype=jnp.int32)
    lower = (position[:, None] >= position[None, :])[None, :, :, None, None]
    weights = jnp.exp(jnp.where(lower, spans, -jnp.inf))
    scores = jnp.einsum("clgn,csgn->clsg", reads, writes, precision=highest)
    inner = jnp.einsum("clsgr,csgrp->clgrp", scores[..., None] * weights, inputs, precision=highest)
    tails = jnp.exp(cumul[:, -1:] - cumul)
    block_states = jnp.einsum(
        "clgn,clgrp->cgrpn", writes, inputs * tails[..., None], precision=highest
    )
    block_decay = jnp.exp(cumul[:, -1])

    def advance(state, pieces):
        factor, added = pieces
        return (factor[..., None, None] * state + added, state)

    final, before = lax.scan(
        advance, entering.reshape(groups, per_group, HEAD_DIM, STATE), (block_decay, block_states)
    )
    carried = (
        jnp.einsum("clgn,cgrpn->clgrp", reads, before, precision=highest)
        * jnp.exp(cumul)[..., None]
    )
    return (
        (inner + carried).reshape(length, heads * HEAD_DIM),
        final.reshape(heads, HEAD_DIM, STATE),
    )


def expert_backward(rows, scaled, gate_weight, up_weight, down_weight):
    gate_pre = jnp.dot(rows, gate_weight, preferred_element_type=jnp.float32)
    up_pre = jnp.dot(rows, up_weight, preferred_element_type=jnp.float32)
    sigma = jax.nn.sigmoid(gate_pre)
    hidden = (jax.nn.silu(gate_pre) * up_pre).astype(jnp.bfloat16)
    over_rows = (((0,), (0,)), ((), ()))
    over_units = (((1,), (1,)), ((), ()))
    grad_down = lax.dot_general(hidden, scaled, over_rows, preferred_element_type=jnp.float32)
    d_hidden = lax.dot_general(scaled, down_weight, over_units, preferred_element_type=jnp.float32)
    d_gate = (d_hidden * up_pre * sigma * (1.0 + gate_pre * (1.0 - sigma))).astype(jnp.bfloat16)
    d_up = (d_hidden * jax.nn.silu(gate_pre)).astype(jnp.bfloat16)
    grad_gate = lax.dot_general(rows, d_gate, over_rows, preferred_element_type=jnp.float32)
    grad_up = lax.dot_general(rows, d_up, over_rows, preferred_element_type=jnp.float32)
    value_portion = lax.dot_general(
        d_gate, gate_weight, over_units, preferred_element_type=jnp.float32
    )
    value_portion = value_portion + lax.dot_general(
        d_up, up_weight, over_units, preferred_element_type=jnp.float32
    )
    return (
        grad_gate.astype(jnp.bfloat16),
        grad_up.astype(jnp.bfloat16),
        grad_down.astype(jnp.bfloat16),
        value_portion,
    )


def body(
    token_values,
    write_keys,
    read_keys,
    log_decay,
    out_gate,
    out_proj,
    mixed,
    cotangent,
    route_ids,
    route_weights,
    w_gate,
    w_up,
    w_down,
):
    tok_rows, width = mixed.shape
    experts = lax.axis_size("sp")
    expert_capacity = 3 * tok_rows // experts
    flat_ids = route_ids.reshape(-1)
    pairs = flat_ids.shape[0]
    member = (flat_ids[:, None] == jnp.arange(experts, dtype=jnp.int32)[None, :]).astype(jnp.int32)
    earlier = jnp.cumsum(member, axis=0) - member
    slot_index = jnp.sum(earlier * member, axis=1)
    target = flat_ids * expert_capacity + slot_index
    copies = jnp.repeat(mixed, 2, axis=0)
    scaled = (cotangent.astype(jnp.float32)[:, None, :] * route_weights[:, :, None]).reshape(
        pairs, width
    )
    scaled = scaled.astype(jnp.bfloat16)
    places = experts * expert_capacity
    share = width // lax.axis_size("tp")
    offset = lax.axis_index("tp") * share
    part_rows = lax.dynamic_slice_in_dim(copies, offset, share, 1)
    part_scaled = lax.dynamic_slice_in_dim(scaled, offset, share, 1)
    send_rows = jnp.zeros((places, share), jnp.bfloat16).at[target].set(part_rows)
    send_scaled = jnp.zeros((places, share), jnp.bfloat16).at[target].set(part_scaled)
    got_pieces = (
        lax.all_to_all(
            send_rows.reshape(experts, expert_capacity, share),
            "sp",
            split_axis=0,
            concat_axis=0,
            tiled=True,
        ),
        lax.all_to_all(
            send_scaled.reshape(experts, expert_capacity, share),
            "sp",
            split_axis=0,
            concat_axis=0,
            tiled=True,
        ),
    )
    got_rows, got_scaled = (
        lax.all_gather(got_pieces[0], "tp", axis=2, tiled=True),
        lax.all_gather(got_pieces[1], "tp", axis=2, tiled=True),
    )
    grads = expert_backward(
        got_rows.reshape(places, width),
        got_scaled.reshape(places, width),
        w_gate[0],
        w_up[0],
        w_down[0],
    )
    summed = lax.psum_scatter(
        grads[3].reshape(experts, expert_capacity, width).astype(jnp.bfloat16),
        "tp",
        scatter_dimension=2,
        tiled=True,
    )
    came = lax.all_to_all(summed, "sp", split_axis=0, concat_axis=0, tiled=True)
    returned = lax.all_gather(came, "tp", axis=2, tiled=True).reshape(places, width)
    picked = jnp.take(returned, target, axis=0).astype(jnp.float32).reshape(tok_rows, 2, width)
    grad_mixed = (cotangent.astype(jnp.float32) + jnp.sum(picked, axis=1)).astype(jnp.bfloat16)
    out_grad = jnp.dot(grad_mixed, out_proj, preferred_element_type=jnp.float32)
    values_float = token_values.astype(jnp.float32)
    writes_float = write_keys.astype(jnp.float32)
    reads_float = read_keys.astype(jnp.float32)
    gate_float = out_gate.astype(jnp.float32)
    heads = log_decay.shape[0]
    groups = write_keys.shape[1] // STATE
    per_group = heads // groups
    cumul = jnp.cumsum(log_decay, axis=1)
    total = cumul[:, -1]
    tails = jnp.exp(total[:, None] - cumul).T.reshape(tok_rows, groups, per_group)
    leads = jnp.exp(cumul).T.reshape(tok_rows, groups, per_group)
    inputs = values_float.reshape(tok_rows, groups, per_group, HEAD_DIM)
    outer_grad = (out_grad * jax.nn.silu(gate_float)).reshape(tok_rows, groups, per_group, HEAD_DIM)
    writes = writes_float.reshape(tok_rows, groups, STATE)
    reads = reads_float.reshape(tok_rows, groups, STATE)
    local_end = jnp.einsum("tgrp,tgn->grpn", inputs * tails[..., None], writes, precision=highest)
    local_back = jnp.einsum(
        "tgrp,tgn->grpn", outer_grad * leads[..., None], reads, precision=highest
    )
    totals, ends, backs = (
        lax.all_gather(total[None].astype(jnp.bfloat16), "sp", axis=0, tiled=True).astype(
            jnp.float32
        ),
        lax.all_gather(local_end[None].astype(jnp.bfloat16), "sp", axis=0, tiled=True).astype(
            jnp.float32
        ),
        lax.all_gather(local_back[None].astype(jnp.bfloat16), "sp", axis=0, tiled=True).astype(
            jnp.float32
        ),
    )
    segments = lax.axis_size("sp")
    own_index = lax.axis_index("sp")
    indices = jnp.arange(segments, dtype=jnp.int32)
    inclusive = jnp.cumsum(totals, axis=0)
    exclusive = inclusive - totals
    own_exclusive = jnp.sum(jnp.where((indices == own_index)[:, None], exclusive, 0.0), axis=0)
    own_inclusive = own_exclusive + total
    earlier_mask = (indices < own_index)[:, None]
    later_mask = (indices > own_index)[:, None]
    up_weight = jnp.exp(jnp.where(earlier_mask, own_exclusive[None, :] - inclusive, -jnp.inf))
    down_weight = jnp.exp(jnp.where(later_mask, exclusive - own_inclusive[None, :], -jnp.inf))
    entering = jnp.einsum(
        "kh,khpn->hpn", up_weight, ends.reshape(segments, heads, HEAD_DIM, STATE), precision=highest
    )
    leaving = jnp.einsum(
        "kh,khpn->hpn",
        down_weight,
        backs.reshape(segments, heads, HEAD_DIM, STATE),
        precision=highest,
    )

    def local_mix(values_in, writes_in, reads_in, gate_in):
        mixed_heads, final = mix_blocks(values_in, writes_in, reads_in, log_decay, entering)
        return (mixed_heads * jax.nn.silu(gate_in), final)

    outputs, pullback = jax.vjp(local_mix, values_float, writes_float, reads_float, gate_float)
    d_values, d_writes, d_reads, d_gate = pullback((out_grad, leaving))
    gated_b = outputs[0].astype(jnp.bfloat16)
    proj_grad = lax.psum_scatter(
        lax.dot_general(
            grad_mixed, gated_b, (((0,), (0,)), ((), ())), preferred_element_type=jnp.float32
        ).astype(jnp.bfloat16),
        "sp",
        scatter_dimension=0,
        tiled=True,
    ).astype(jnp.float32)
    return (
        d_values.astype(jnp.bfloat16),
        d_writes.astype(jnp.bfloat16),
        d_reads.astype(jnp.bfloat16),
        d_gate.astype(jnp.bfloat16),
        proj_grad,
        grads[0][None],
        grads[1][None],
        grads[2][None],
    )


def solution(mesh):
    return jax.shard_map(
        body,
        mesh=mesh,
        in_specs=(
            P("sp", "tp"),
            P("sp", "tp"),
            P("sp", "tp"),
            P("tp", "sp"),
            P("sp", "tp"),
            P(None, "tp"),
            P("sp", None),
            P("sp", None),
            P("sp", None),
            P("sp", None),
            P("sp", None, "tp"),
            P("sp", None, "tp"),
            P("sp", "tp", None),
        ),
        out_specs=(
            P("sp", "tp"),
            P("sp", "tp"),
            P("sp", "tp"),
            P("sp", "tp"),
            P("sp", "tp"),
            P("sp", None, "tp"),
            P("sp", None, "tp"),
            P("sp", "tp", None),
        ),
        check_vma=False,
    )
```

profile of v0, /device:TPU:0, one launch (start us, length us, event | category | flops | bytes accessed | tf_op | source)
XLA Modules:
  0.0 392.4 jit_solution(12014310925594720735)
XLA Ops:
  7.2 0.8 broadcast_multiply_fusion
  8.1 0.8 copy.123
  9.5 1.2 reduce-window.16
  11.2 6.0 %broadcast_in_dim.110 = bf16[256,2,4096]{2,1,0:T(2,128)(2,1)} broadcast(bf16[256,4096]{1,0:T(8,128)(2,1)} %param.23), dimensions={0,2} | broadcast | bytes 6291456 | tf_op jit(solution)/shard_map/broadcast_in_dim | solution.py:105
  17.2 7.3 %reshape.395 = bf16[512,4096]{1,0:T(8,128)(2,1)} reshape(bf16[256,2,4096]{2,1,0:T(2,128)(2,1)} %broadcast_in_dim.110) | data formatting | bytes 8388608 | tf_op jit(solution)/shard_map/reshape | solution.py:105
  24.5 3.1 scatter_custom_fusion.1
  27.6 26.4 %all_to_all.15 = bf16[4,192,512]{2,1,0:T(8,128)(2,1)} all-to-all(bf16[4,192,512]{2,1,0:T(8,128)(2,1)S(1)} %bitcast.285), channel_id=1, replica_groups=mesh['sp'=4,'tp'=8] {'sp'}, dimensions={0} | all-to-all | bytes 1572864 | tf_op jit(solution)/shard_map/all_to_all | solution.py:118
  54.4 8.3 %mul.225 = f32[256,2,4096]{2,1,0:T(2,128)} broadcast(bf16[256,4096]{1,0:T(8,128)(2,1)} %param.24), dimensions={0,2} | broadcast | bytes 10485760 | tf_op jit(solution)/shard_map/mul | solution.py:106
  62.7 10.9 %mul.226 = f32[512,4096]{1,0:T(8,128)} reshape(f32[256,2,4096]{2,1,0:T(2,128)} %mul.225) | data formatting | bytes 16777216 | tf_op jit(solution)/shard_map/mul | solution.py:106
  73.6 3.4 scatter_custom_fusion
  77.0 22.4 %all_to_all.16 = bf16[4,192,512]{2,1,0:T(8,128)(2,1)} all-to-all(bf16[4,192,512]{2,1,0:T(8,128)(2,1)S(1)} %bitcast.284), channel_id=1, replica_groups=mesh['sp'=4,'tp'=8] {'sp'}, dimensions={0} | all-to-all | bytes 1572864 | tf_op jit(solution)/shard_map/all_to_all | solution.py:125
  99.9 4.7 %fusion.7 = f32[768,256]{1,0:T(8,128)S(1)} fusion(bf16[768,4096]{1,0:T(8,128)(2,1)} %bitcast.313, bf16[1,4096,256]{2,1,0:T(8,128)(2,1)S(1)} %copy-done), kind=kOutput, calls=%fused_computation.25 | convolution fusion | flops 1610612736 | bytes 9175040 | tf_op jit(solution)/shard_map/dot_general | solution.py:55
  105.1 2.7 fusion.10
  107.8 40.6 %all-gather.7.cloned.1.call-done = bf16[4,192,4096]{2,1,0:T(8,128)(2,1)} async-done(((bf16[4,192,512]{2,1,0:T(8,128)(2,1)}), bf16[4,192,4096]{2,1,0:T(8,128)(2,1)}) %all-gather.7.cloned.1.call-update) | async-done | bytes 6291472 | tf_op jit(solution)/shard_map/all_gather | solution.py:135
  148.4 5.5 %multiply_convert_fusion.1 = (bf16[768,256]{1,0:T(8,128)(2,1)S(1)}, bf16[768,256]{1,0:T(8,128)(2,1)S(1)}) fusion(f32[768,256]{1,0:T(8,128)S(1)} %fusion.7, f32[768,256]{1,0:T(8,128)} %fusion.10, bf16[768,4096]{1,0:T(8,128)(2,1)} %bitcast.278, bf16[1,256,4096]{2,1,0:T(8,128)(2,1)} %param.29), kind=kOutput, calls=%fused_computation.59 | convolution fusion | flops 1613168640 | bytes 10747904 | tf_op jit(solution)/shard_map/dot_general | solution.py:62
  153.9 1.8 fusion.5
  155.8 4.5 %add_convert_fusion = bf16[768,4096]{1,0:T(8,128)(2,1)} fusion(f32[768,4096]{1,0:T(8,128)S(1)} %fusion.5, bf16[768,256]{1,0:T(8,128)(2,1)S(1)} %get-tuple-element.249, bf16[1,4096,256]{2,1,0:T(8,128)(2,1)S(1)} %copy-done.9), kind=kOutput, calls=%fused_computation.12 | convolution fusion | flops 1616904192 | bytes 21364736 | tf_op jit(solution)/shard_map/dot_general | solution.py:70
  160.4 61.7 %reduce-scatter.3.cloned.1.call-done = bf16[4,192,512]{2,1,0:T(8,128)(2,1)} async-done(((bf16[4,192,4096]{2,1,0:T(8,128)(2,1)}), bf16[4,192,512]{2,1,0:T(8,128)(2,1)}) %reduce-scatter.3.cloned.1.call-update) | async-done | bytes 786448 | tf_op jit(solution)/shard_map/reduce_scatter | solution.py:144
  222.1 24.6 %all_to_all.17 = bf16[4,192,512]{2,1,0:T(8,128)(2,1)} all-to-all(bf16[4,192,512]{2,1,0:T(8,128)(2,1)} %reduce-scatter.3.cloned.1.call-done), channel_id=1, replica_groups=mesh['sp'=4,'tp'=8] {'sp'}, dimensions={0} | all-to-all | bytes 1572864 | tf_op jit(solution)/shard_map/all_to_all | solution.py:150
  246.9 1.2 reduce-window.14
  248.7 0.6 dynamic-slice
  250.2 9.8 %all-reduce = bf16[16]{0:T(256)(128)(2,1)S(1)} all-reduce(bf16[16]{0:T(256)(128)(2,1)S(1)} %dynamic-update-slice), channel_id=2, replica_groups=mesh['sp'=4,'tp'=8] {'sp'}, use_global_device_ids=true, to_apply=%add | all-reduce | flops 16 | bytes 64
  261.0 0.6 copy.150
  262.8 0.6 exponential_bitcast_fusion
  264.0 13.9 %all-gather.2 = bf16[16,64,128]{2,1,0:T(8,128)(2,1)S(1)} all-gather(bf16[4,64,128]{2,1,0:T(8,128)(2,1)S(1)} %convolution_convert_fusion.4), channel_id=4, replica_groups=mesh['sp'=4,'tp'=8] {'sp'}, dimensions={0}, use_global_device_ids=true | all-gather | bytes 327680 | tf_op jit(solution)/shard_map/all_gather | solution.py:178
  277.9 0.7 convolution_bitcast_fusion.4
  278.7 0.5 convolution_bitcast_fusion.1
  279.3 0.6 fusion.63
  279.9 2.9 while.30
  280.8 0.5 constant_dynamic-update-slice_fusion.2
  282.1 0.6 constant_dynamic-update-slice_fusion.2
  282.9 0.9 fusion.17
  284.4 6.1 %fusion.3 = bf16[1,4096,256]{2,1,0:T(8,128)(2,1)} fusion(bf16[768,4096]{1,0:T(8,128)(2,1)} %bitcast.314, bf16[768,256]{1,0:T(8,128)(2,1)S(1)} %copy-done.17), kind=kOutput, calls=%fused_computation.20 | convolution fusion | flops 1611661312 | bytes 8781824 | tf_op jit(solution)/shard_map/dot_general | solution.py:66
  290.5 6.1 %fusion.2 = bf16[1,4096,256]{2,1,0:T(8,128)(2,1)} fusion(bf16[768,4096]{1,0:T(8,128)(2,1)} %bitcast.315, bf16[768,256]{1,0:T(8,128)(2,1)S(1)} %copy-done.15), kind=kOutput, calls=%fused_computation.19 | convolution fusion | flops 1611661312 | bytes 8781824 | tf_op jit(solution)/shard_map/dot_general | solution.py:65
  296.7 3.2 fusion.4
  299.9 12.2 %gather_fusion = bf16[512,4096]{1,0:T(8,128)(2,1)} fusion(bf16[768,4096]{1,0:T(8,128)(2,1)} %bitcast.276, s32[1024]{0:T(1024)S(1)} %pad_clamp_fusion), kind=kCustom, calls=%fused_computation | custom fusion | bytes 8390656 | tf_op jit(solution)/shard_map/jit(_take)/gather | solution.py:152
  312.1 7.7 %gather.7 = bf16[256,2,4096]{2,1,0:T(2,128)(2,1)} reshape(bf16[512,4096]{1,0:T(8,128)(2,1)} %gather_fusion) | data formatting | bytes 8388608 | tf_op jit(solution)/shard_map/jit(_take)/gather | solution.py:152
  319.8 14.3 %convert_reduce_fusion = f32[256,4096]{1,0:T(8,128)S(1)} fusion(bf16[256,2,4096]{2,1,0:T(2,128)(2,1)} %gather.7, pred[256,2]{1,0:T(8,128)(4,1)S(1)} %copy.126), kind=kLoop, calls=%fused_computation.13 | loop fusion | flops 5242880 | bytes 8389120 | tf_op jit(solution)/shard_map/reduce_sum | solution.py:153
  334.1 1.9 copy-done.2
  336.0 2.5 convolution_convert_fusion
  338.5 3.8 bitcast_multiply_fusion.1
  342.6 0.8 copy.149
  343.9 16.2 %all-gather.1 = bf16[16,64,128]{2,1,0:T(8,128)(2,1)S(1)} all-gather(bf16[4,64,128]{2,1,0:T(8,128)(2,1)S(1)} %convolution_convert_fusion.5), channel_id=3, replica_groups=mesh['sp'=4,'tp'=8] {'sp'}, dimensions={0}, use_global_device_ids=true | all-gather | bytes 327680 | tf_op jit(solution)/shard_map/all_gather | solution.py:181
  360.1 0.7 convolution_bitcast_fusion.5
  360.8 2.9 convolution_bitcast_fusion.6
  363.7 0.6 fusion.65
  364.3 0.9 broadcast.196
  365.2 5.6 %while.31 = (s32[]{:T(128)}, f32[1,4,64,128]{3,2,1,0:T(8,128)S(1)}, f32[4,1,4,64,128]{4,3,2,1,0:T(8,128)}, f32[4,1,4,64,128]{4,3,2,1,0:T(8,128)S(1)}, f32[4,1,4,1,1]{2,4,3,1,0:T(1,128)}, /*index=5*/s32[]{:T(128)}, s32[]{:T(128)}) while((s32[]{:T(128)}, f32[1,4,64,128]{3,2,1,0:T(8,128)S(1)}, f32[4,1,4,64,128]{4,3,2,1,0:T(8,128)}, ...), condition=%wide.region_15.16_spmd, body=%wide.region_14.15_spmd.sunk | while | flops 65539 | bytes 655509 | solution.py:41
  365.2 0.7 fusion.116
  365.9 0.7 bitcast_dynamic-update-slice_fusion.5
  366.6 0.6 fusion.116
  367.2 0.7 bitcast_dynamic-update-slice_fusion.5
  368.0 0.6 fusion.116
  368.6 0.7 bitcast_dynamic-update-slice_fusion.5
  369.4 0.6 fusion.116
  370.0 0.7 bitcast_dynamic-update-slice_fusion.5
  370.8 2.4 fusion.19
  373.2 1.8 copy.143
  375.0 1.8 convert_element_type.134
  376.9 1.5 fusion.20
  378.7 0.8 convolution_bitcast_fusion.7
  379.4 0.8 fusion.23
  380.3 2.9 fusion.22
  383.4 2.1 convert_element_type.142
  (157 shorter events, 9.8 us)
Async XLA Ops:
  7.2 92.7 %copy-start = (bf16[1,4096,256]{2,1,0:T(8,128)(2,1)S(1)}, bf16[1,4096,256]{2,1,0:T(8,128)(2,1)}, u32[]{:S(2)}) copy-start(bf16[1,4096,256]{2,1,0:T(8,128)(2,1)} %param.27) | copy-start | bytes 6291460
  7.2 92.7 %all-gather.9.cloned.1.call-start = ((), (), s32[]{:S(2)}) async-start(), calls=%async_computation.6 | async-start | bytes 7077888 | tf_op jit(solution)/shard_map/all_gather | solution.py:134
  17.2 36.9 %copy-start.26 = (f32[256,2]{0,1:T(2,128)S(1)}, f32[256,2]{0,1:T(2,128)}, u32[]{:S(2)}) copy-start(f32[256,2]{0,1:T(2,128)} %param.26) | copy-start | bytes 6148
  54.0 94.3 %all-gather.7.cloned.1.call-start = ((), (), s32[]{:S(2)}) async-start(), calls=%async_computation.5 | async-start | bytes 7077888 | tf_op jit(solution)/shard_map/all_gather | solution.py:135
  99.4 122.7 %reduce-scatter.3.cloned.1.call-start = ((), (), s32[]{:S(2)}) async-start(), calls=%async_computation.7 | async-start | bytes 7077888 | tf_op jit(solution)/shard_map/reduce_scatter | solution.py:144
  99.9 4.7 %copy-start.8 = (bf16[1,4096,256]{2,1,0:T(8,128)(2,1)S(1)}, bf16[1,4096,256]{2,1,0:T(8,128)(2,1)}, u32[]{:S(2)}) copy-start(bf16[1,4096,256]{2,1,0:T(8,128)(2,1)} %param.28) | copy-start | bytes 6291460
  99.9 5.2 %copy-start.28 = (bf16[4,192,4096]{2,1,0:T(8,128)(2,1)S(1)}, bf16[4,192,4096]{2,1,0:T(8,128)(2,1)}, u32[]{:S(2)}) copy-start(bf16[4,192,4096]{2,1,0:T(8,128)(2,1)} %all-gather.9.cloned.1.call-done) | copy-start | bytes 18874372
  105.1 43.2 %copy-start.5 = (f32[768,256]{1,0:T(8,128)}, f32[768,256]{1,0:T(8,128)S(1)}, u32[]{:S(2)}) copy-start(f32[768,256]{1,0:T(8,128)S(1)} %fusion.7) | copy-start | bytes 2359300
  153.9 1.9 copy-start.14
  153.9 1.9 copy-start.16
  153.9 1.9 copy-start.9
  160.3 86.5 %copy-start.25 = (f32[4,256]{1,0:T(4,128)S(1)}, f32[4,256]{1,0:T(4,128)}, u32[]{:S(2)}) copy-start(f32[4,256]{1,0:T(4,128)} %param.20) | copy-start | bytes 12292
  160.3 88.4 %copy-start.29 = (u32[32]{0:T(128)S(1)}, u32[32]{0:T(128)}, u32[]{:S(2)}) copy-start(u32[32]{0:T(128)} %constant.119) | copy-start | bytes 388
  160.3 100.0 %copy-start.12 = (bf16[256,256]{1,0:T(8,128)(2,1)S(1)}, bf16[256,256]{1,0:T(8,128)(2,1)}, u32[]{:S(2)}) copy-start(bf16[256,256]{1,0:T(8,128)(2,1)} %param.17) | copy-start | bytes 393220
  160.3 101.4 %copy-start.21 = (bf16[256,256]{1,0:T(8,128)(2,1)S(1)}, bf16[256,256]{1,0:T(8,128)(2,1)}, u32[]{:S(2)}) copy-start(bf16[256,256]{1,0:T(8,128)(2,1)} %param.21) | copy-start | bytes 393220
  160.3 101.5 %copy-start.24 = (s32[256,2]{0,1:T(2,128)S(1)}, s32[256,2]{0,1:T(2,128)}, u32[]{:S(2)}) copy-start(s32[256,2]{0,1:T(2,128)} %param.25) | copy-start | bytes 6148
  160.3 101.9 %copy-start.10 = (bf16[256,128]{1,0:T(8,128)(2,1)S(1)}, bf16[256,128]{1,0:T(8,128)(2,1)}, u32[]{:S(2)}) copy-start(bf16[256,128]{1,0:T(8,128)(2,1)} %param.19) | copy-start | bytes 196612
  160.3 101.9 %copy-start.11 = (bf16[256,128]{1,0:T(8,128)(2,1)S(1)}, bf16[256,128]{1,0:T(8,128)(2,1)}, u32[]{:S(2)}) copy-start(bf16[256,128]{1,0:T(8,128)(2,1)} %param.18) | copy-start | bytes 196612
  160.4 139.5 %all-gather.11.cloned.1.call-start = ((), (), s32[]{:S(2)}) async-start(), calls=%async_computation.8 | async-start | bytes 7077888 | tf_op jit(solution)/shard_map/all_gather | solution.py:151
  246.8 136.6 %reduce-scatter.5.cloned.1.call-start = ((), (), s32[]{:S(2)}) async-start(), calls=%async_computation.9 | async-start | bytes 2621440 | tf_op jit(solution)/shard_map/reduce_scatter | solution.py:213
  260.5 18.2 %copy-start.18 = (bf16[4,64,4,64]{3,2,1,0:T(4,128)(2,1)}, bf16[4,64,4,64]{3,2,1,0:T(4,128)(2,1)S(1)}, u32[]{:S(2)}) copy-start(bf16[4,64,4,64]{3,2,1,0:T(4,128)(2,1)S(1)} %reshape.411) | copy-start | bytes 393220
  262.3 17.6 %copy-start.19 = (f32[4,64,1,4]{1,3,0,2:T(4,128)}, f32[4,64,1,4]{1,3,0,2:T(4,128)S(1)}, u32[]{:S(2)}) copy-start(f32[4,64,1,4]{1,3,0,2:T(4,128)S(1)} %copy.131) | copy-start | bytes 12292
  262.5 17.3 %copy-start.13 = (f32[4,64,64]{2,1,0:T(8,128)}, f32[4,64,64]{2,1,0:T(8,128)S(1)}, u32[]{:S(2)}) copy-start(f32[4,64,64]{2,1,0:T(8,128)S(1)} %copy.141) | copy-start | bytes 196612
  263.7 15.6 %copy-start.4 = (f32[4,64,4,64]{3,1,2,0:T(8,128)}, f32[4,64,4,64]{3,1,2,0:T(8,128)S(1)}, u32[]{:S(2)}) copy-start(f32[4,64,4,64]{3,1,2,0:T(8,128)S(1)} %copy.135) | copy-start | bytes 786436
  277.8 6.2 %copy-start.22 = (pred[64,64]{1,0:T(8,128)(4,1)}, pred[64,64]{1,0:T(8,128)(4,1)S(1)}, u32[]{:S(2)}) copy-start(pred[64,64]{1,0:T(8,128)(4,1)S(1)} %iota_compare_fusion) | copy-start | bytes 12292
  279.3 5.1 %copy-start.17 = (bf16[768,256]{1,0:T(8,128)(2,1)S(1)}, bf16[768,256]{1,0:T(8,128)(2,1)}, u32[]{:S(2)}) copy-start(bf16[768,256]{1,0:T(8,128)(2,1)} %copy-done.16) | copy-start | bytes 1179652
  284.4 6.2 %copy-start.15 = (bf16[768,256]{1,0:T(8,128)(2,1)S(1)}, bf16[768,256]{1,0:T(8,128)(2,1)}, u32[]{:S(2)}) copy-start(bf16[768,256]{1,0:T(8,128)(2,1)} %copy-done.14) | copy-start | bytes 1179652
  284.4 12.3 %slice-start = ((s8[6291456]{0:T(1024)(128)(4,1)}), s8[4194304]{0:T(1024)(128)(4,1)S(1)}, s32[]{:S(2)}) async-start(s8[6291456]{0:T(1024)(128)(4,1)} %bitcast.279), calls=%async_computation.10 | async-start | bytes 8388608
  290.5 6.1 %slice-start.1 = ((s8[6291456]{0:T(1024)(128)(4,1)}), s8[2097152]{0:T(1024)(128)(4,1)S(1)}, s32[]{:S(2)}) async-start(s8[6291456]{0:T(1024)(128)(4,1)} %bitcast.279), calls=%async_computation.11 | async-start | bytes 4194304
  290.5 6.1 %copy-start.6 = (f32[768,256]{1,0:T(8,128)S(1)}, f32[768,256]{1,0:T(8,128)}, u32[]{:S(2)}) copy-start(f32[768,256]{1,0:T(8,128)} %copy-done.5) | copy-start | bytes 2359300
  290.5 6.1 %copy-start.7 = (f32[768,256]{1,0:T(8,128)S(1)}, f32[768,256]{1,0:T(8,128)}, u32[]{:S(2)}) copy-start(f32[768,256]{1,0:T(8,128)} %fusion.10) | copy-start | bytes 2359300
  319.7 16.3 %copy-start.3 = (bf16[256,4096]{1,0:T(8,128)(2,1)S(1)}, bf16[256,4096]{1,0:T(8,128)(2,1)}, u32[]{:S(2)}) copy-start(bf16[256,4096]{1,0:T(8,128)(2,1)} %param.24) | copy-start | bytes 6291460
  334.1 2.0 copy-start.2
  342.3 21.4 %copy-start.27 = (f32[4,4,1,1]{0,2,3,1:T(1,128)S(1)}, f32[4,4,1,1]{0,2,3,1:T(1,128)}, u32[]{:S(2)}) copy-start(f32[4,4,1,1]{0,2,3,1:T(1,128)} %copy.150) | copy-start | bytes 196
  360.8 16.0 %copy-start.20 = (f32[4,64,1,4]{1,3,0,2:T(4,128)S(1)}, f32[4,64,1,4]{1,3,0,2:T(4,128)}, u32[]{:S(2)}) copy-start(f32[4,64,1,4]{1,3,0,2:T(4,128)} %copy-done.19) | copy-start | bytes 12292
  360.8 16.0 %copy-start.23 = (pred[64,64]{1,0:T(8,128)(4,1)S(1)}, pred[64,64]{1,0:T(8,128)(4,1)}, u32[]{:S(2)}) copy-start(pred[64,64]{1,0:T(8,128)(4,1)} %copy-done.22) | copy-start | bytes 12292
  370.8 14.7 %copy-start.1 = (bf16[1,4096,256]{2,1,0:T(8,128)(2,1)S(1)}, bf16[1,4096,256]{2,1,0:T(8,128)(2,1)}, u32[]{:S(2)}) copy-start(bf16[1,4096,256]{2,1,0:T(8,128)(2,1)} %param.27) | copy-start | bytes 6291460
Sparse Core Ops, SparseCore 0:
  54.2 45.6 all-gather.8
  101.7 46.5 all-gather.6
  160.5 61.5 reduce-scatter.2
  246.9 44.7 all-gather.10
  338.6 44.6 reduce-scatter.4
where the time goes:
time: 400 us; the launch traced here: 392 us
  blocking collectives  113 us (28%)
  waiting for transfers between devices  103 us (26%)
  local copies, waits for them, and re-layouts  77.4 us (19%)
  matrix products  57.4 us (14%)
  other arithmetic  25.3 us (6%)
  between operations  15.5 us (4%)
    reduce_scatter x1, waiting for transfers between devices, body(): lax.psum_scatter(grads[3].reshape(experts, expert_capacity, width).astype...  61.7 us
    all_gather x1, waiting for transfers between devices, body(): lax.all_gather(got_pieces[1], 'tp', axis=2, tiled=True)  40.6 us
    all_to_all x1, blocking collectives, body(): lax.all_to_all(send_rows.reshape(experts, expert_capacity, share), 'sp',...  26.4 us
    all_to_all x1, blocking collectives, body(): came = lax.all_to_all(summed, 'sp', split_axis=0, concat_axis=0, tiled=True)  24.6 us
    all_to_all x1, blocking collectives, body(): lax.all_to_all(send_scaled.reshape(experts, expert_capacity, share), 'sp'...  22.4 us
    gather x2, local copies, waits for them, and re-layouts, body(): jnp.take(returned, target, axis=0).astype(jnp.float32)  19.8 us
    mul x3, local copies, waits for them, and re-layouts, body(): cotangent.astype(jnp.float32)[:, None, :] * route_weights[:, :, None]  19.4 us
    all_gather x1, blocking collectives, body(): lax.all_gather(local_back[None].astype(jnp.bfloat16), 'sp', axis=0, tiled...  16.2 us
  transfers between devices with their start and end apart: 5, of which 4 were waited for; matrix products, arithmetic and copies ran while one was open for 22% of the time, Pallas kernels for 0%

commit v1 on v0

v1 whole, which is shorter than its diff:
```python
import jax
import jax.numpy as jnp
from jax import lax
from jax.sharding import PartitionSpec as P

HEAD_DIM = 64
STATE = 128

F32 = jnp.float32
BF16 = jnp.bfloat16


def dot(a, b, ca=1, cb=0):
    return lax.dot_general(a, b, (((ca,), (cb,)), ((), ())), preferred_element_type=F32)


def shift(x, by):
    n = lax.axis_size("sp")
    return lax.ppermute(x, "sp", [(i, (i + by) % n) for i in range(n)])


def body(
    token_values,
    write_keys,
    read_keys,
    log_decay,
    out_gate,
    out_proj,
    mixed,
    cotangent,
    route_ids,
    route_weights,
    w_gate,
    w_up,
    w_down,
):
    tok, width = mixed.shape
    n = lax.axis_size("sp")
    cap = 3 * tok // n
    share = width // lax.axis_size("tp")
    own = lax.axis_index("sp")
    offset = lax.axis_index("tp") * share

    rel = lax.rem(route_ids - own + n, n)
    hit = rel[:, :, None] == jnp.arange(n, dtype=jnp.int32)[None, None, :]
    member = jnp.any(hit, axis=1)
    weight = jnp.sum(jnp.where(hit, route_weights[:, :, None], 0.0), axis=1)
    order = jnp.arange(tok, dtype=jnp.int32)
    before = (order[:, None] > order[None, :]).astype(BF16)
    slot = dot(before, member.astype(BF16)).astype(jnp.int32)
    slot = jnp.where(member, slot, -1).T
    place = jnp.arange(cap, dtype=jnp.int32)
    chosen = slot[:, None, :] == place[None, :, None]
    onehot = chosen.astype(BF16)
    row_weight = jnp.sum(jnp.where(chosen, weight.T[:, None, :], 0.0), axis=2)

    mixed_part = lax.dynamic_slice_in_dim(mixed, offset, share, 1)
    cot_part = lax.dynamic_slice_in_dim(cotangent, offset, share, 1)
    away = onehot[1:].reshape((n - 1) * cap, tok)
    away_weight = row_weight[1:].reshape((n - 1) * cap, 1)
    send_rows = dot(away, mixed_part).astype(BF16).reshape(n - 1, cap, share)
    send_scaled = (dot(away, cot_part) * away_weight).astype(BF16).reshape(n - 1, cap, share)
    got_rows = jnp.concatenate([shift(send_rows[j - 1], j) for j in range(1, n)], axis=0)
    got_scaled = jnp.concatenate([shift(send_scaled[j - 1], j) for j in range(1, n)], axis=0)
    rem_rows = lax.all_gather(got_rows, "tp", axis=1, tiled=True)
    rem_scaled = lax.all_gather(got_scaled, "tp", axis=1, tiled=True)
    loc_rows = dot(onehot[0], mixed).astype(BF16)
    loc_scaled = (dot(onehot[0], cotangent) * row_weight[0][:, None]).astype(BF16)

    heads = log_decay.shape[0]
    groups = write_keys.shape[1] // STATE
    per_group = heads // groups
    cumul = jnp.cumsum(log_decay, axis=1)
    total = cumul[:, -1]
    tails = jnp.exp(total[:, None] - cumul)
    leads = jnp.exp(cumul)
    values = token_values.astype(F32)
    gate = out_gate.astype(F32)
    sig = jax.nn.sigmoid(gate)
    silu = gate * sig
    causal = order[:, None] >= order[None, :]

    def widen(per_head):
        return jnp.repeat(per_head.T, HEAD_DIM, axis=1)

    tails_wide = widen(tails)
    leads_wide = widen(leads)
    tailed = (values * tails_wide).astype(BF16)

    def cols(a, g):
        k = per_group * HEAD_DIM
        return a[:, g * k : (g + 1) * k]

    def keys(a, g):
        return a[:, g * STATE : (g + 1) * STATE]

    def head(a, h):
        return a[:, h * HEAD_DIM : (h + 1) * HEAD_DIM]

    local_end = jnp.concatenate(
        [dot(cols(tailed, g), keys(write_keys, g), 0, 0) for g in range(groups)], axis=0
    )
    packed = jnp.concatenate(
        [local_end, jnp.broadcast_to(total[:, None], (heads, STATE))], axis=0
    ).astype(BF16)
    lengths = heads * HEAD_DIM
    entering = jnp.zeros((lengths, STATE), F32)
    run = jnp.zeros((heads,), F32)
    for j in range(1, n):
        got = shift(packed, j).astype(F32)
        live = own >= j
        factor = jnp.where(live, jnp.exp(run), 0.0)
        entering = entering + jnp.repeat(factor, HEAD_DIM)[:, None] * got[:lengths]
        run = run + jnp.where(live, got[lengths:, 0], 0.0)
    ahead = [shift(packed[lengths:], -j).astype(F32)[:, 0] for j in range(1, n)]
    entering_b = entering.astype(BF16)

    decay_of, kept, outs = [], [], []
    scores = [dot(keys(read_keys, g), keys(write_keys, g), 1, 1) for g in range(groups)]
    for h in range(heads):
        span = cumul[h][:, None] - cumul[h][None, :]
        decay = jnp.exp(jnp.where(causal, span, -jnp.inf))
        decay_of.append(decay)
        kept.append((scores[h // per_group] * decay).astype(BF16))
        outs.append(dot(kept[h], head(token_values, h)))
    carried = jnp.concatenate(
        [
            dot(keys(read_keys, g), entering_b[g * per_group * HEAD_DIM : (g + 1) * per_group * HEAD_DIM], 1, 1)
            for g in range(groups)
        ],
        axis=1,
    )
    y = jnp.concatenate(outs, axis=1) + carried * leads_wide
    gated_b = (y * silu).astype(BF16)

    def both(loc, rem, w, cb):
        return jnp.concatenate([dot(loc, w, 1, cb), dot(rem, w, 1, cb)], axis=0)

    def over_rows(loc, rem, d):
        return (dot(loc, d[:cap], 0, 0) + dot(rem, d[cap:], 0, 0)).astype(BF16)

    gate_pre = both(loc_rows, rem_rows, w_gate[0], 0)
    up_pre = both(loc_rows, rem_rows, w_up[0], 0)
    sigma = jax.nn.sigmoid(gate_pre)
    act_gate = gate_pre * sigma
    hidden = (act_gate * up_pre).astype(BF16)
    d_hidden = both(loc_scaled, rem_scaled, w_down[0], 1)
    d_gate = (d_hidden * up_pre * sigma * (1.0 + gate_pre * (1.0 - sigma))).astype(BF16)
    d_up = (d_hidden * act_gate).astype(BF16)
    portion = (dot(d_gate, w_gate[0], 1, 1) + dot(d_up, w_up[0], 1, 1)).astype(BF16)
    summed = lax.psum_scatter(portion, "tp", scatter_dimension=1, tiled=True)
    grad_gate = over_rows(loc_rows, rem_rows, d_gate)
    grad_up = over_rows(loc_rows, rem_rows, d_up)
    grad_down = (
        dot(hidden[:cap], loc_scaled, 0, 0) + dot(hidden[cap:], rem_scaled, 0, 0)
    ).astype(BF16)

    came = [summed[:cap]] + [
        shift(summed[j * cap : (j + 1) * cap], -j) for j in range(1, n)
    ]
    came = jnp.concatenate(came, axis=0)
    back = dot(onehot.reshape(n * cap, tok), came, 0, 0)
    grad_part = (cot_part.astype(F32) + back).astype(BF16)
    grad_mixed = lax.all_gather(grad_part, "tp", axis=1, tiled=True)

    out_grad = dot(grad_mixed, out_proj)
    proj_part = dot(grad_mixed, gated_b, 0, 0).astype(BF16)
    proj_grad = lax.psum_scatter(proj_part, "sp", scatter_dimension=0, tiled=True).astype(F32)

    outer = out_grad * silu
    outer_b = outer.astype(BF16)
    led = (outer * leads_wide).astype(BF16)
    local_back = jnp.concatenate(
        [dot(cols(led, g), keys(read_keys, g), 0, 0) for g in range(groups)], axis=0
    ).astype(BF16)
    leaving = jnp.zeros((lengths, STATE), F32)
    run = jnp.zeros((heads,), F32)
    for j in range(1, n):
        got = shift(local_back, -j).astype(F32)
        live = own + j < n
        factor = jnp.where(live, jnp.exp(run), 0.0)
        leaving = leaving + jnp.repeat(factor, HEAD_DIM)[:, None] * got
        run = run + jnp.where(live, ahead[j - 1], 0.0)
    leaving_b = leaving.astype(BF16)

    d_values, d_writes, d_reads = [], [], []
    for g in range(groups):
        d_scores = 0.0
        for r in range(per_group):
            h = g * per_group + r
            d_scores = d_scores + dot(head(outer_b, h), head(token_values, h), 1, 1) * decay_of[h]
            d_values.append(dot(kept[h], head(outer_b, h), 0, 0))
        d_scores = d_scores.astype(BF16)
        span = slice(g * per_group * HEAD_DIM, (g + 1) * per_group * HEAD_DIM)
        d_reads.append(dot(d_scores, keys(write_keys, g)) + dot(led[:, span], entering_b[span]))
        d_writes.append(
            dot(d_scores, keys(read_keys, g), 0, 0) + dot(tailed[:, span], leaving_b[span])
        )
    from_end = jnp.concatenate(
        [
            dot(keys(write_keys, g), leaving_b[g * per_group * HEAD_DIM : (g + 1) * per_group * HEAD_DIM], 1, 1)
            for g in range(groups)
        ],
        axis=1,
    )
    d_values = jnp.concatenate(d_values, axis=1) + from_end * tails_wide
    d_out_gate = out_grad * y * sig * (1.0 + gate * (1.0 - sig))
    return (
        d_values.astype(BF16),
        jnp.concatenate(d_writes, axis=1).astype(BF16),
        jnp.concatenate(d_reads, axis=1).astype(BF16),
        d_out_gate.astype(BF16),
        proj_grad,
        grad_gate[None],
        grad_up[None],
        grad_down[None],
    )


def solution(mesh):
    return jax.shard_map(
        body,
        mesh=mesh,
        in_specs=(
            P("sp", "tp"),
            P("sp", "tp"),
            P("sp", "tp"),
            P("tp", "sp"),
            P("sp", "tp"),
            P(None, "tp"),
            P("sp", None),
            P("sp", None),
            P("sp", None),
            P("sp", None),
            P("sp", None, "tp"),
            P("sp", None, "tp"),
            P("sp", "tp", None),
        ),
        out_specs=(
            P("sp", "tp"),
            P("sp", "tp"),
            P("sp", "tp"),
            P("sp", "tp"),
            P("sp", "tp"),
            P("sp", None, "tp"),
            P("sp", None, "tp"),
            P("sp", "tp", None),
        ),
        check_vma=False,
    )
```

time: 400 us -> 303 us (0.76); the launches traced: 392 us -> 303 us
  blocking collectives: 113 us -> 0 us
  waiting for transfers between devices: 103 us -> 170 us
  local copies, waits for them, and re-layouts: 77.4 us -> 10.9 us
  starting transfers between devices: 0.38 us -> 36.9 us
  other arithmetic: 25.3 us -> 12.4 us
    all_to_all x3 -> x0, blocking collectives: 73.4 us -> none  [the longest x1 26.4 us: body(): lax.all_to_all(send_rows.reshape(experts, expert_capacity, share), 'sp',...]
    ppermute x0 -> x17, waiting for transfers between devices: none -> 38.5 us  [shift(): return lax.ppermute(x, 'sp', [(i, (i + by) % n) for i in range(n)])]
    ppermute x0 -> x17, starting transfers between devices: none -> 36.7 us  [shift(): return lax.ppermute(x, 'sp', [(i, (i + by) % n) for i in range(n)])]
    all_gather x2 -> x0, blocking collectives: 30.1 us -> none  [the longest x1 16.2 us: body(): lax.all_gather(local_back[None].astype(jnp.bfloat16), 'sp', axis=0, tiled...]
    mul x14 -> x5, local copies, waits for them, and re-layouts: 22.3 us -> 0.99 us  [the longest x2 0.74 us: body(): leaving = leaving + jnp.repeat(factor, HEAD_DIM)[:, None] * got]
    gather x2 -> x0, local copies, waits for them, and re-layouts: 19.8 us -> none  [body(): jnp.take(returned, target, axis=0).astype(jnp.float32)]
    reduce_scatter x2, waiting for transfers between devices: 61.9 us -> 77.9 us  [the longest x1 53.8 us: body(): summed = lax.psum_scatter(portion, 'tp', scatter_dimension=1, tiled=True)]
    reduce_sum x3 -> x2, other arithmetic: 14.4 us -> 0.23 us  [the longest x1 0.22 us: body(): row_weight = jnp.sum(jnp.where(chosen, weight.T[:, None, :], 0.0), axis=2)]
  transfers between devices with their start and end apart: 5 -> 22, of which waited for: 4 -> 13; matrix products, arithmetic and copies ran while one was open for 22% -> 18% of each run, Pallas kernels for 0% -> 0%
where the time goes in v1:
time: 303 us
  waiting for transfers between devices  170 us (56%)
  matrix products  58 us (19%)
  starting transfers between devices  36.9 us (12%)
  between operations  14.5 us (5%)
  other arithmetic  12.4 us (4%)
  local copies, waits for them, and re-layouts  10.9 us (4%)
    dot_general x43, matrix products, dot(): lax.dot_general(a, b, (((ca,), (cb,)), ((), ())), preferred_element_type=...  58 us
    reduce_scatter x1, waiting for transfers between devices, body(): summed = lax.psum_scatter(portion, 'tp', scatter_dimension=1, tiled=True)  53.8 us
    ppermute x17, waiting for transfers between devices, shift(): return lax.ppermute(x, 'sp', [(i, (i + by) % n) for i in range(n)])  38.5 us
    ppermute x17, starting transfers between devices, shift(): return lax.ppermute(x, 'sp', [(i, (i + by) % n) for i in range(n)])  36.7 us
    all_gather x1, waiting for transfers between devices, body(): rem_scaled = lax.all_gather(got_scaled, 'tp', axis=1, tiled=True)  34 us
    reduce_scatter x1, waiting for transfers between devices, body(): lax.psum_scatter(proj_part, 'sp', scatter_dimension=0, tiled=True)  24.1 us
    all_gather x1, waiting for transfers between devices, body(): rem_rows = lax.all_gather(got_rows, 'tp', axis=1, tiled=True)  14.3 us
    unnamed x86, local copies, waits for them, and re-layouts  7.65 us
  transfers between devices with their start and end apart: 22, of which 13 were waited for; matrix products, arithmetic and copies ran while one was open for 18% of the time, Pallas kernels for 0%

profile of v1, /device:TPU:0, one launch (start us, length us, event | category | flops | bytes accessed | tf_op | source)
XLA Modules:
  0.0 302.8 jit_solution(12068777380833281221)
XLA Ops:
  7.2 0.8 compare_select_fusion
  8.5 1.3 convolution_convert_fusion.2
  9.8 3.1 %collective-permute-start.3 = (bf16[192,512]{1,0:T(8,128)(2,1)S(1)}, bf16[192,512]{1,0:T(8,128)(2,1)S(1)}, u32[]{:S(2)}, u32[]{:S(2)}) collective-permute-start(bf16[192,512]{1,0:T(8,128)(2,1)S(1)} %get-tuple-element.46), channel_id=1, source_target_pairs={{0,8},{8,16},{16,24},{24,0},{1,9},{9,17},{17,25},{25,1},{2,10},{10... | collective-permute-start | bytes 589832 | tf_op jit(solution)/shard_map/ppermute | solution.py:19
  13.0 2.6 collective-permute-start.4
  15.5 1.3 collective-permute-start.5
  16.9 4.0 %collective-permute-done.3 = bf16[192,512]{1,0:T(8,128)(2,1)S(1)} collective-permute-done((bf16[192,512]{1,0:T(8,128)(2,1)S(1)}, bf16[192,512]{1,0:T(8,128)(2,1)S(1)}, u32[]{:S(2)}, u32[]{:S(2)}) %collective-permute-start.3) | collective-permute-done | bytes 196640 | tf_op jit(solution)/shard_map/ppermute | solution.py:19
  20.9 7.6 %collective-permute-done.4 = bf16[192,512]{1,0:T(8,128)(2,1)S(1)} collective-permute-done((bf16[192,512]{1,0:T(8,128)(2,1)S(1)}, bf16[192,512]{1,0:T(8,128)(2,1)S(1)}, u32[]{:S(2)}, u32[]{:S(2)}) %collective-permute-start.4) | collective-permute-done | bytes 196640 | tf_op jit(solution)/shard_map/ppermute | solution.py:19
  28.4 0.9 pad_maximum_fusion.4
  29.7 1.3 fusion.22
  31.0 4.7 %collective-permute-start = (bf16[192,512]{1,0:T(8,128)(2,1)S(1)}, bf16[192,512]{1,0:T(8,128)(2,1)S(1)}, u32[]{:S(2)}, u32[]{:S(2)}) collective-permute-start(bf16[192,512]{1,0:T(8,128)(2,1)S(1)} %get-tuple-element.43), channel_id=1, source_target_pairs={{0,8},{8,16},{16,24},{24,0},{1,9},{9,17},{17,25},{25,1},{2,10},{10... | collective-permute-start | bytes 589832 | tf_op jit(solution)/shard_map/ppermute | solution.py:19
  35.8 1.6 collective-permute-start.1
  37.4 0.8 collective-permute-start.2
  38.2 4.5 %collective-permute-done = bf16[192,512]{1,0:T(8,128)(2,1)S(1)} collective-permute-done((bf16[192,512]{1,0:T(8,128)(2,1)S(1)}, bf16[192,512]{1,0:T(8,128)(2,1)S(1)}, u32[]{:S(2)}, u32[]{:S(2)}) %collective-permute-start) | collective-permute-done | bytes 196640 | tf_op jit(solution)/shard_map/ppermute | solution.py:19
  42.7 6.7 %collective-permute-done.1 = bf16[192,512]{1,0:T(8,128)(2,1)S(1)} collective-permute-done((bf16[192,512]{1,0:T(8,128)(2,1)S(1)}, bf16[192,512]{1,0:T(8,128)(2,1)S(1)}, u32[]{:S(2)}, u32[]{:S(2)}) %collective-permute-start.1) | collective-permute-done | bytes 196640 | tf_op jit(solution)/shard_map/ppermute | solution.py:19
  49.4 0.9 pad_maximum_fusion.3
  50.3 2.3 convolution_convert_fusion.1
  54.0 1.7 copy-done.7
  56.3 1.1 copy-done.11
  57.4 0.8 fusion.20
  58.2 14.3 %all-gather.6.cloned.1.call-done = bf16[576,4096]{1,0:T(8,128)(2,1)} async-done(((bf16[576,512]{1,0:T(8,128)(2,1)}), bf16[576,4096]{1,0:T(8,128)(2,1)}) %all-gather.6.cloned.1.call-update) | async-done | bytes 4718608 | tf_op jit(solution)/shard_map/all_gather | solution.py:65
  72.5 5.4 %fusion.14 = f32[576,256]{1,0:T(8,128)} fusion(bf16[576,4096]{1,0:T(8,128)(2,1)} %all-gather.6.cloned.1.call-done, bf16[1,4096,256]{2,1,0:T(8,128)(2,1)} %param.24), kind=kOutput, calls=%fused_computation.21 | convolution fusion | flops 1207959552 | bytes 7405568 | tf_op jit(solution)/shard_map/dot_general | solution.py:14
  77.8 2.2 fusion.9
  80.1 34.0 %all-gather.4.cloned.1.call-done = bf16[576,4096]{1,0:T(8,128)(2,1)} async-done(((bf16[576,512]{1,0:T(8,128)(2,1)}), bf16[576,4096]{1,0:T(8,128)(2,1)}) %all-gather.4.cloned.1.call-update) | async-done | bytes 4718608 | tf_op jit(solution)/shard_map/all_gather | solution.py:66
  114.0 4.5 %fusion.18 = f32[576,256]{1,0:T(8,128)S(1)} fusion(bf16[576,4096]{1,0:T(8,128)(2,1)} %all-gather.4.cloned.1.call-done, bf16[1,256,4096]{2,1,0:T(8,128)(2,1)} %param.25), kind=kOutput, calls=%fused_computation.25 | convolution fusion | flops 1207959552 | bytes 7405568 | tf_op jit(solution)/shard_map/dot_general | solution.py:14
  118.6 1.2 multiply_convert_fusion
  119.8 1.8 fusion.7
  121.6 5.5 %add_convert_fusion = bf16[768,4096]{1,0:T(8,128)(2,1)} fusion(f32[768,4096]{1,0:T(8,128)S(1)} %fusion.7, bf16[768,256]{1,0:T(8,128)(2,1)} %get-tuple-element.38, bf16[1,4096,256]{2,1,0:T(8,128)(2,1)S(1)} %copy-done.8), kind=kOutput, calls=%fused_computation | convolution fusion | flops 1616904192 | bytes 21364736 | tf_op jit(solution)/shard_map/dot_general | solution.py:14
  127.9 1.2 reduce-window.6
  130.8 1.5 collective-permute-start.14
  132.3 2.4 collective-permute-start.15
  135.2 53.8 %reduce-scatter.3.cloned.1.call-done = bf16[768,512]{1,0:T(8,128)(2,1)} async-done(((bf16[768,4096]{1,0:T(8,128)(2,1)}), bf16[768,512]{1,0:T(8,128)(2,1)}) %reduce-scatter.3.cloned.1.call-update) | async-done | bytes 786448 | tf_op jit(solution)/shard_map/reduce_scatter | solution.py:151
  189.0 1.3 fusion.99
  190.2 3.4 %collective-permute-start.6 = (bf16[192,512]{1,0:T(8,128)(2,1)S(1)}, bf16[192,512]{1,0:T(8,128)(2,1)S(1)}, u32[]{:S(2)}, u32[]{:S(2)}) collective-permute-start(bf16[192,512]{1,0:T(8,128)(2,1)S(1)} %get-tuple-element.42), channel_id=1, source_target_pairs={{0,24},{8,0},{16,8},{24,16},{1,25},{9,1},{17,9},{25,17},{2,26},{10... | collective-permute-start | bytes 589832 | tf_op jit(solution)/shard_map/ppermute | solution.py:19
  193.6 1.1 collective-permute-start.8
  194.8 4.2 %collective-permute-done.6 = bf16[192,512]{1,0:T(8,128)(2,1)S(1)} collective-permute-done((bf16[192,512]{1,0:T(8,128)(2,1)S(1)}, bf16[192,512]{1,0:T(8,128)(2,1)S(1)}, u32[]{:S(2)}, u32[]{:S(2)}) %collective-permute-start.6) | collective-permute-done | bytes 196640 | tf_op jit(solution)/shard_map/ppermute | solution.py:19
  199.0 4.3 %collective-permute-start.16 = (bf16[260,128]{1,0:T(8,128)(2,1)}, bf16[260,128]{1,0:T(8,128)(2,1)}, u32[]{:S(2)}, u32[]{:S(2)}) collective-permute-start(bf16[260,128]{1,0:T(8,128)(2,1)} %pad_maximum_fusion.5), channel_id=1, source_target_pairs={{0,24},{8,0},{16,8},{24,16},{1,25},{9,1},{17,9},{25,17},{2,26},{10... | collective-permute-start | bytes 199688 | tf_op jit(solution)/shard_map/ppermute | solution.py:19
  203.3 7.8 %collective-permute-done.7 = bf16[192,512]{1,0:T(8,128)(2,1)S(1)} collective-permute-done((bf16[192,512]{1,0:T(8,128)(2,1)S(1)}, bf16[192,512]{1,0:T(8,128)(2,1)S(1)}, u32[]{:S(2)}, u32[]{:S(2)}) %collective-permute-start.7) | collective-permute-done | bytes 196640 | tf_op jit(solution)/shard_map/ppermute | solution.py:19
  211.2 3.3 %collective-permute-start.12 = (bf16[4,128]{1,0:T(4,128)(2,1)S(1)}, bf16[4,128]{1,0:T(4,128)(2,1)}, u32[]{:S(2)}, u32[]{:S(2)}) collective-permute-start(bf16[4,128]{1,0:T(4,128)(2,1)S(1)} %broadcast_in_dim.99), channel_id=1, source_target_pairs={{0,16},{8,24},{16,0},{24,8},{1,17},{9,25},{17,1},{25,9},{2,18},{10... | collective-permute-start | bytes 3080 | tf_op jit(solution)/shard_map/ppermute | solution.py:19
  214.5 2.1 fusion.23
  216.7 0.9 fusion.66
  217.6 0.9 fusion.69
  218.5 0.9 fusion.72
  219.5 0.9 fusion.75
  220.3 1.0 copy.41
  221.4 0.8 select_reduce_fusion.4
  223.1 0.9 convert_element_type.152
  224.0 0.9 convert_element_type.153
  226.0 1.1 fusion.59
  227.1 1.3 fusion.25
  230.7 3.2 %fusion.4 = bf16[1,256,4096]{2,1,0:T(8,128)(2,1)} fusion(f32[256,4096]{1,0:T(8,128)S(1)} %fusion.60, bf16[576,4096]{1,0:T(8,128)(2,1)S(1)} %bitcast.122, bf16[768,256]{1,0:T(8,128)(2,1)S(1)} %get-tuple-element.36), kind=kOutput, calls=%fused_computation.11 | convolution fusion | flops 1210056704 | bytes 11304960 | tf_op jit(solution)/shard_map/dot_general | solution.py:14
  233.9 3.2 %fusion.5 = bf16[1,4096,256]{2,1,0:T(8,128)(2,1)} fusion(f32[4096,256]{1,0:T(8,128)S(1)} %fusion.62, bf16[576,4096]{1,0:T(8,128)(2,1)S(1)} %bitcast.133, bf16[768,256]{1,0:T(8,128)(2,1)S(1)} %copy-done.12), kind=kOutput, calls=%fused_computation.12 | convolution fusion | flops 1210056704 | bytes 11304960 | tf_op jit(solution)/shard_map/dot_general | solution.py:14
  237.1 5.4 %all-gather.8.cloned.1.call-done = bf16[256,4096]{1,0:T(8,128)(2,1)} async-done(((bf16[256,512]{1,0:T(8,128)(2,1)}), bf16[256,4096]{1,0:T(8,128)(2,1)}) %all-gather.8.cloned.1.call-update) | async-done | bytes 2097168 | tf_op jit(solution)/shard_map/all_gather | solution.py:164
  242.5 3.7 %convolution_convert_fusion = bf16[4096,256]{1,0:T(8,128)(2,1)} fusion(bf16[256,4096]{1,0:T(8,128)(2,1)} %all-gather.8.cloned.1.call-done, f32[256,256]{0,1:T(8,128)S(1)} %fusion.25, bf16[256,256]{0,1:T(8,128)(2,1)S(1)} %copy.41), kind=kOutput, calls=%fused_computation.8 | convolution fusion | flops 538378240 | bytes 4587520 | tf_op jit(solution)/shard_map/dot_general | solution.py:14
  247.0 5.7 %fusion.6 = bf16[1,4096,256]{2,1,0:T(8,128)(2,1)} fusion(f32[4096,256]{1,0:T(8,128)S(1)} %fusion.64, bf16[576,4096]{1,0:T(8,128)(2,1)} %all-gather.6.cloned.1.call-done, bf16[768,256]{1,0:T(8,128)(2,1)S(1)} %get-tuple-element.37), kind=kOutput, calls=%fused_computation.13 | convolution fusion | flops 1210056704 | bytes 11304960 | tf_op jit(solution)/shard_map/dot_general | solution.py:14
  252.8 0.9 fusion.52
  253.9 2.5 collective-permute-start.11
  256.4 1.5 collective-permute-start.13
  257.9 2.3 collective-permute-start.9
  262.4 0.9 fusion.34
  264.3 2.0 collective-permute-done.11
  266.2 1.8 collective-permute-done.9
  269.1 0.9 fusion.33
  270.1 24.1 %reduce-scatter.5.cloned.1.call-done = bf16[1024,256]{1,0:T(8,128)(2,1)} async-done(((bf16[4096,256]{1,0:T(8,128)(2,1)}), bf16[1024,256]{1,0:T(8,128)(2,1)}) %reduce-scatter.5.cloned.1.call-update) | async-done | bytes 524304 | tf_op jit(solution)/shard_map/reduce_scatter | solution.py:168
  294.2 2.1 convert_element_type.159
  (166 shorter events, 15.3 us)
Async XLA Ops:
  7.2 46.1 %copy-start = (bf16[1,4096,256]{2,1,0:T(8,128)(2,1)S(1)}, bf16[1,4096,256]{2,1,0:T(8,128)(2,1)}, u32[]{:S(2)}) copy-start(bf16[1,4096,256]{2,1,0:T(8,128)(2,1)} %param.23) | copy-start | bytes 6291460
  7.2 65.3 %all-gather.6.cloned.1.call-start = ((), (), s32[]{:S(2)}) async-start(), calls=%async_computation.3 | async-start | bytes 5308416 | tf_op jit(solution)/shard_map/all_gather | solution.py:65
  8.4 21.0 %copy-start.30 = (f32[256,2]{0,1:T(2,128)S(1)}, f32[256,2]{0,1:T(2,128)}, u32[]{:S(2)}) copy-start(f32[256,2]{0,1:T(2,128)} %param.22) | copy-start | bytes 6148
  9.8 11.0 %collective-permute-start.3 = (bf16[192,512]{1,0:T(8,128)(2,1)S(1)}, bf16[192,512]{1,0:T(8,128)(2,1)S(1)}, u32[]{:S(2)}, u32[]{:S(2)}) collective-permute-start(bf16[192,512]{1,0:T(8,128)(2,1)S(1)} %get-tuple-element.46), channel_id=1, source_target_pairs={{0,8},{8,16},{16,24},{24,0},{1,9},{9,17},{17,25},{25,1},{2,10},{10... | collective-permute-start | bytes 589832 | tf_op jit(solution)/shard_map/ppermute | solution.py:19
  13.0 15.5 %collective-permute-start.4 = (bf16[192,512]{1,0:T(8,128)(2,1)S(1)}, bf16[192,512]{1,0:T(8,128)(2,1)S(1)}, u32[]{:S(2)}, u32[]{:S(2)}) collective-permute-start(bf16[192,512]{1,0:T(8,128)(2,1)S(1)} %get-tuple-element.48), channel_id=1, source_target_pairs={{0,16},{8,24},{16,0},{24,8},{1,17},{9,25},{17,1},{25,9},{2,18},{10... | collective-permute-start | bytes 589832 | tf_op jit(solution)/shard_map/ppermute | solution.py:19
  15.5 12.9 %collective-permute-start.5 = (bf16[192,512]{1,0:T(8,128)(2,1)S(1)}, bf16[192,512]{1,0:T(8,128)(2,1)S(1)}, u32[]{:S(2)}, u32[]{:S(2)}) collective-permute-start(bf16[192,512]{1,0:T(8,128)(2,1)S(1)} %get-tuple-element.47), channel_id=1, source_target_pairs={{0,24},{8,0},{16,8},{24,16},{1,25},{9,1},{17,9},{25,17},{2,26},{10... | collective-permute-start | bytes 589832 | tf_op jit(solution)/shard_map/ppermute | solution.py:19
  29.3 84.7 %all-gather.4.cloned.1.call-start = ((), (), s32[]{:S(2)}) async-start(), calls=%async_computation.2 | async-start | bytes 5308416 | tf_op jit(solution)/shard_map/all_gather | solution.py:66
  31.0 11.6 %collective-permute-start = (bf16[192,512]{1,0:T(8,128)(2,1)S(1)}, bf16[192,512]{1,0:T(8,128)(2,1)S(1)}, u32[]{:S(2)}, u32[]{:S(2)}) collective-permute-start(bf16[192,512]{1,0:T(8,128)(2,1)S(1)} %get-tuple-element.43), channel_id=1, source_target_pairs={{0,8},{8,16},{16,24},{24,0},{1,9},{9,17},{17,25},{25,1},{2,10},{10... | collective-permute-start | bytes 589832 | tf_op jit(solution)/shard_map/ppermute | solution.py:19
  35.8 13.6 %collective-permute-start.1 = (bf16[192,512]{1,0:T(8,128)(2,1)S(1)}, bf16[192,512]{1,0:T(8,128)(2,1)S(1)}, u32[]{:S(2)}, u32[]{:S(2)}) collective-permute-start(bf16[192,512]{1,0:T(8,128)(2,1)S(1)} %get-tuple-element.45), channel_id=1, source_target_pairs={{0,16},{8,24},{16,0},{24,8},{1,17},{9,25},{17,1},{25,9},{2,18},{10... | collective-permute-start | bytes 589832 | tf_op jit(solution)/shard_map/ppermute | solution.py:19
  37.4 12.0 %collective-permute-start.2 = (bf16[192,512]{1,0:T(8,128)(2,1)S(1)}, bf16[192,512]{1,0:T(8,128)(2,1)S(1)}, u32[]{:S(2)}, u32[]{:S(2)}) collective-permute-start(bf16[192,512]{1,0:T(8,128)(2,1)S(1)} %get-tuple-element.44), channel_id=1, source_target_pairs={{0,24},{8,0},{16,8},{24,16},{1,25},{9,1},{17,9},{25,17},{2,26},{10... | collective-permute-start | bytes 589832 | tf_op jit(solution)/shard_map/ppermute | solution.py:19
  50.3 138.7 %reduce-scatter.3.cloned.1.call-start = ((), (), s32[]{:S(2)}) async-start(), calls=%async_computation.4 | async-start | bytes 7077888 | tf_op jit(solution)/shard_map/reduce_scatter | solution.py:151
  50.3 2.4 copy-start.9
  52.7 1.3 copy-start.2
  53.3 3.0 copy-start.5
  53.3 2.4 copy-start.7
  55.7 1.7 copy-start.11
  72.5 5.4 %copy-start.35 = (bf16[576,4096]{1,0:T(8,128)(2,1)S(1)}, bf16[576,4096]{1,0:T(8,128)(2,1)}, u32[]{:S(2)}) copy-start(bf16[576,4096]{1,0:T(8,128)(2,1)} %all-gather.6.cloned.1.call-done) | copy-start | bytes 14155780
  114.0 4.5 %copy-start.15 = (f32[576,256]{1,0:T(8,128)S(1)}, f32[576,256]{1,0:T(8,128)}, u32[]{:S(2)}) copy-start(f32[576,256]{1,0:T(8,128)} %fusion.14) | copy-start | bytes 1769476
  114.0 4.5 %copy-start.16 = (f32[576,256]{1,0:T(8,128)S(1)}, f32[576,256]{1,0:T(8,128)}, u32[]{:S(2)}) copy-start(f32[576,256]{1,0:T(8,128)} %fusion.9) | copy-start | bytes 1769476
  119.8 1.8 copy-start.8
  127.2 0.7 copy-start.29
  127.2 2.5 copy-start.20
  127.2 2.7 copy-start.14
  127.2 7.8 %copy-start.13 = (bf16[256,128]{1,0:T(8,128)(2,1)S(1)}, bf16[256,128]{1,0:T(8,128)(2,1)}, u32[]{:S(2)}) copy-start(bf16[256,128]{1,0:T(8,128)(2,1)} %param.15) | copy-start | bytes 196612
  127.2 115.3 %all-gather.8.cloned.1.call-start = ((), (), s32[]{:S(2)}) async-start(), calls=%async_computation.5 | async-start | bytes 2359296 | tf_op jit(solution)/shard_map/all_gather | solution.py:164
  130.8 92.3 %collective-permute-start.14 = (bf16[260,128]{1,0:T(8,128)(2,1)}, bf16[260,128]{1,0:T(8,128)(2,1)}, u32[]{:S(2)}, u32[]{:S(2)}) collective-permute-start(bf16[260,128]{1,0:T(8,128)(2,1)} %pad_maximum_fusion.5), channel_id=1, source_target_pairs={{0,8},{8,16},{16,24},{24,0},{1,9},{9,17},{17,25},{25,1},{2,10},{10... | collective-permute-start | bytes 199688 | tf_op jit(solution)/shard_map/ppermute | solution.py:19
  132.3 91.7 %collective-permute-start.15 = (bf16[260,128]{1,0:T(8,128)(2,1)}, bf16[260,128]{1,0:T(8,128)(2,1)}, u32[]{:S(2)}, u32[]{:S(2)}) collective-permute-start(bf16[260,128]{1,0:T(8,128)(2,1)} %pad_maximum_fusion.5), channel_id=1, source_target_pairs={{0,16},{8,24},{16,0},{24,8},{1,17},{9,25},{17,1},{25,9},{2,18},{10... | collective-permute-start | bytes 199688 | tf_op jit(solution)/shard_map/ppermute | solution.py:19
  135.2 84.3 %copy-start.22 = (f32[256,256]{1,0:T(8,128)}, f32[256,256]{1,0:T(8,128)S(1)}, u32[]{:S(2)}) copy-start(f32[256,256]{1,0:T(8,128)S(1)} %fusion.102) | copy-start | bytes 786436
  190.2 8.7 %collective-permute-start.6 = (bf16[192,512]{1,0:T(8,128)(2,1)S(1)}, bf16[192,512]{1,0:T(8,128)(2,1)S(1)}, u32[]{:S(2)}, u32[]{:S(2)}) collective-permute-start(bf16[192,512]{1,0:T(8,128)(2,1)S(1)} %get-tuple-element.42), channel_id=1, source_target_pairs={{0,24},{8,0},{16,8},{24,16},{1,25},{9,1},{17,9},{25,17},{2,26},{10... | collective-permute-start | bytes 589832 | tf_op jit(solution)/shard_map/ppermute | solution.py:19
  193.6 17.4 %collective-permute-start.7 = (bf16[192,512]{1,0:T(8,128)(2,1)S(1)}, bf16[192,512]{1,0:T(8,128)(2,1)S(1)}, u32[]{:S(2)}, u32[]{:S(2)}) collective-permute-start(bf16[192,512]{1,0:T(8,128)(2,1)S(1)} %get-tuple-element.41), channel_id=1, source_target_pairs={{0,16},{8,24},{16,0},{24,8},{1,17},{9,25},{17,1},{25,9},{2,18},{10... | collective-permute-start | bytes 589832 | tf_op jit(solution)/shard_map/ppermute | solution.py:19
  193.6 17.6 %collective-permute-start.8 = (bf16[192,512]{1,0:T(8,128)(2,1)S(1)}, bf16[192,512]{1,0:T(8,128)(2,1)S(1)}, u32[]{:S(2)}, u32[]{:S(2)}) collective-permute-start(bf16[192,512]{1,0:T(8,128)(2,1)S(1)} %get-tuple-element.40), channel_id=1, source_target_pairs={{0,8},{8,16},{16,24},{24,0},{1,9},{9,17},{17,25},{25,1},{2,10},{10... | collective-permute-start | bytes 589832 | tf_op jit(solution)/shard_map/ppermute | solution.py:19
  199.0 27.1 %collective-permute-start.16 = (bf16[260,128]{1,0:T(8,128)(2,1)}, bf16[260,128]{1,0:T(8,128)(2,1)}, u32[]{:S(2)}, u32[]{:S(2)}) collective-permute-start(bf16[260,128]{1,0:T(8,128)(2,1)} %pad_maximum_fusion.5), channel_id=1, source_target_pairs={{0,24},{8,0},{16,8},{24,16},{1,25},{9,1},{17,9},{25,17},{2,26},{10... | collective-permute-start | bytes 199688 | tf_op jit(solution)/shard_map/ppermute | solution.py:19
  211.1 10.3 %collective-permute-start.10 = (bf16[4,128]{1,0:T(4,128)(2,1)S(1)}, bf16[4,128]{1,0:T(4,128)(2,1)}, u32[]{:S(2)}, u32[]{:S(2)}) collective-permute-start(bf16[4,128]{1,0:T(4,128)(2,1)S(1)} %broadcast_in_dim.99), channel_id=1, source_target_pairs={{0,24},{8,0},{16,8},{24,16},{1,25},{9,1},{17,9},{25,17},{2,26},{10... | collective-permute-start | bytes 3080 | tf_op jit(solution)/shard_map/ppermute | solution.py:19
  211.2 10.2 %collective-permute-start.12 = (bf16[4,128]{1,0:T(4,128)(2,1)S(1)}, bf16[4,128]{1,0:T(4,128)(2,1)}, u32[]{:S(2)}, u32[]{:S(2)}) collective-permute-start(bf16[4,128]{1,0:T(4,128)(2,1)S(1)} %broadcast_in_dim.99), channel_id=1, source_target_pairs={{0,16},{8,24},{16,0},{24,8},{1,17},{9,25},{17,1},{25,9},{2,18},{10... | collective-permute-start | bytes 3080 | tf_op jit(solution)/shard_map/ppermute | solution.py:19
  216.6 11.8 %copy-start.3 = (bf16[192,4096]{1,0:T(8,128)(2,1)S(1)}, bf16[192,4096]{1,0:T(8,128)(2,1)}, u32[]{:S(2)}) copy-start(bf16[192,4096]{1,0:T(8,128)(2,1)} %copy-done.2) | copy-start | bytes 4718596
  216.6 11.8 %copy-start.12 = (bf16[768,256]{1,0:T(8,128)(2,1)S(1)}, bf16[768,256]{1,0:T(8,128)(2,1)}, u32[]{:S(2)}) copy-start(bf16[768,256]{1,0:T(8,128)(2,1)} %get-tuple-element.38) | copy-start | bytes 1179652
  216.6 77.6 %reduce-scatter.5.cloned.1.call-start = ((), (), s32[]{:S(2)}) async-start(), calls=%async_computation.6 | async-start | bytes 2621440 | tf_op jit(solution)/shard_map/reduce_scatter | solution.py:168
  216.7 3.7 %copy-start.25 = (f32[256]{0:T(256)}, f32[256]{0:T(256)S(1)}, u32[]{:S(2)}) copy-start(f32[256]{0:T(256)S(1)} %get-tuple-element.54) | copy-start | bytes 3076
  216.7 3.6 %copy-start.27 = (f32[256]{0:T(256)}, f32[256]{0:T(256)S(1)}, u32[]{:S(2)}) copy-start(f32[256]{0:T(256)S(1)} %get-tuple-element.55) | copy-start | bytes 3076
  216.7 3.6 %copy-start.31 = (f32[256]{0:T(256)}, f32[256]{0:T(256)S(1)}, u32[]{:S(2)}) copy-start(f32[256]{0:T(256)S(1)} %get-tuple-element.53) | copy-start | bytes 3076
  216.7 3.6 %copy-start.33 = (f32[256]{0:T(256)}, f32[256]{0:T(256)S(1)}, u32[]{:S(2)}) copy-start(f32[256]{0:T(256)S(1)} %get-tuple-element.52) | copy-start | bytes 3076
  224.9 0.7 copy-start.19
  227.1 2.2 copy-start.17
  227.1 3.5 %slice-start = ((s8[4718592]{0:T(1024)(128)(4,1)}), s8[4194304]{0:T(1024)(128)(4,1)S(1)}, s32[]{:S(2)}) async-start(s8[4718592]{0:T(1024)(128)(4,1)} %bitcast.121), calls=%async_computation.7 | async-start | bytes 8388608
  228.4 1.5 copy-start.6
  228.4 2.2 slice-start.1
  229.9 3.9 %slice-start.2 = ((s8[4718592]{0:T(1024)(128)(4,1)}), s8[4194304]{0:T(1024)(128)(4,1)S(1)}, s32[]{:S(2)}) async-start(s8[4718592]{0:T(1024)(128)(4,1)} %bitcast.132), calls=%async_computation.9 | async-start | bytes 8388608
  230.7 3.2 %slice-start.3 = ((s8[4718592]{0:T(1024)(128)(4,1)}), s8[524288]{0:T(1024)(128)(4,1)S(1)}, s32[]{:S(2)}) async-start(s8[4718592]{0:T(1024)(128)(4,1)} %bitcast.132), calls=%async_computation.10 | async-start | bytes 1048576
  247.0 5.7 %copy-start.4 = (bf16[256,4096]{1,0:T(8,128)(2,1)S(1)}, bf16[256,4096]{1,0:T(8,128)(2,1)}, u32[]{:S(2)}) copy-start(bf16[256,4096]{1,0:T(8,128)(2,1)} %all-gather.8.cloned.1.call-done) | copy-start | bytes 6291460
  247.0 5.7 %copy-start.10 = (bf16[4096,256]{1,0:T(8,128)(2,1)S(1)}, bf16[4096,256]{1,0:T(8,128)(2,1)}, u32[]{:S(2)}) copy-start(bf16[4096,256]{1,0:T(8,128)(2,1)} %param.18) | copy-start | bytes 6291460
  252.7 7.5 %copy-start.21 = (bf16[256,256]{1,0:T(8,128)(2,1)S(1)}, bf16[256,256]{1,0:T(8,128)(2,1)}, u32[]{:S(2)}) copy-start(bf16[256,256]{1,0:T(8,128)(2,1)} %param.13) | copy-start | bytes 393220
  252.7 7.5 %copy-start.34 = (f32[256]{0:T(256)S(1)}, f32[256]{0:T(256)}, u32[]{:S(2)}) copy-start(f32[256]{0:T(256)} %copy-done.33) | copy-start | bytes 3076
  252.7 7.7 %copy-start.28 = (f32[256]{0:T(256)S(1)}, f32[256]{0:T(256)}, u32[]{:S(2)}) copy-start(f32[256]{0:T(256)} %copy-done.27) | copy-start | bytes 3076
  252.7 8.0 %copy-start.26 = (f32[256]{0:T(256)S(1)}, f32[256]{0:T(256)}, u32[]{:S(2)}) copy-start(f32[256]{0:T(256)} %copy-done.25) | copy-start | bytes 3076
  252.8 8.2 %copy-start.32 = (f32[256]{0:T(256)S(1)}, f32[256]{0:T(256)}, u32[]{:S(2)}) copy-start(f32[256]{0:T(256)} %copy-done.31) | copy-start | bytes 3076
  253.7 7.7 %copy-start.23 = (f32[256,256]{1,0:T(8,128)S(1)}, f32[256,256]{1,0:T(8,128)}, u32[]{:S(2)}) copy-start(f32[256,256]{1,0:T(8,128)} %copy-done.22) | copy-start | bytes 786436
  253.9 12.3 %collective-permute-start.11 = (bf16[256,128]{1,0:T(8,128)(2,1)S(1)}, bf16[256,128]{1,0:T(8,128)(2,1)S(1)}, u32[]{:S(2)}, u32[]{:S(2)}) collective-permute-start(bf16[256,128]{1,0:T(8,128)(2,1)S(1)} %convolution_convert_fusion.4), channel_id=1, source_target_pairs={{0,16},{8,24},{16,0},{24,8},{1,17},{9,25},{17,1},{25,9},{2,18},{10... | collective-permute-start | bytes 196616 | tf_op jit(solution)/shard_map/ppermute | solution.py:19
  256.4 9.8 %collective-permute-start.13 = (bf16[256,128]{1,0:T(8,128)(2,1)S(1)}, bf16[256,128]{1,0:T(8,128)(2,1)S(1)}, u32[]{:S(2)}, u32[]{:S(2)}) collective-permute-start(bf16[256,128]{1,0:T(8,128)(2,1)S(1)} %convolution_convert_fusion.4), channel_id=1, source_target_pairs={{0,8},{8,16},{16,24},{24,0},{1,9},{9,17},{17,25},{25,1},{2,10},{10... | collective-permute-start | bytes 196616 | tf_op jit(solution)/shard_map/ppermute | solution.py:19
  257.9 10.2 %collective-permute-start.9 = (bf16[256,128]{1,0:T(8,128)(2,1)S(1)}, bf16[256,128]{1,0:T(8,128)(2,1)S(1)}, u32[]{:S(2)}, u32[]{:S(2)}) collective-permute-start(bf16[256,128]{1,0:T(8,128)(2,1)S(1)} %convolution_convert_fusion.4), channel_id=1, source_target_pairs={{0,24},{8,0},{16,8},{24,16},{1,25},{9,1},{17,9},{25,17},{2,26},{10... | collective-permute-start | bytes 196616 | tf_op jit(solution)/shard_map/ppermute | solution.py:19
  260.2 2.2 copy-start.18
  261.0 7.1 %copy-start.24 = (f32[256]{0:T(256)S(1)}, f32[256]{0:T(256)}, u32[]{:S(2)}) copy-start(f32[256]{0:T(256)} %mul.182) | copy-start | bytes 3076
  262.4 33.9 %copy-start.1 = (bf16[1,4096,256]{2,1,0:T(8,128)(2,1)S(1)}, bf16[1,4096,256]{2,1,0:T(8,128)(2,1)}, u32[]{:S(2)}) copy-start(bf16[1,4096,256]{2,1,0:T(8,128)(2,1)} %param.23) | copy-start | bytes 6291460
Sparse Core Ops, SparseCore 0:
  29.4 43.0 all-gather.5
  74.4 39.6 all-gather.3
  127.3 61.5 reduce-scatter.2
  216.7 25.7 all-gather.7
  246.3 47.8 reduce-scatter.4

commit v2 on v1

--- a/solution.py
+++ b/solution.py
@@ -1,6 +1,10 @@
+import functools
+
 import jax
 import jax.numpy as jnp
 from jax import lax
+from jax.experimental import pallas as pl
+from jax.experimental.pallas import tpu as pltpu
 from jax.sharding import PartitionSpec as P
 
 HEAD_DIM = 64
@@ -17,6 +21,112 @@
 def shift(x, by):
     n = lax.axis_size("sp")
     return lax.ppermute(x, "sp", [(i, (i + by) % n) for i in range(n)])
+
+
+def spread_kernel(n, arrays, far, *refs):
+    sends, outs = refs[:arrays], refs[arrays : 2 * arrays]
+    send_sem, recv_sem, local_sem = refs[2 * arrays :]
+    t = lax.axis_index("tp")
+    s = lax.axis_index("sp")
+    blocks, rows, cols = sends[0].shape
+    half = rows // 2
+    chunks = [(a, j) for a in range(arrays) for j in range(blocks)]
+    near = [{"tp": t ^ bit} for bit in (1, 2, 4)]
+    other, across, along = near
+    peers = list(near)
+    if far:
+        peers += [{"sp": lax.rem(s + j, n)} for j in range(1, n)]
+    barrier = pltpu.get_barrier_semaphore()
+    for peer in peers:
+        pl.semaphore_signal(barrier, inc=1, device_id=peer, device_id_type=pl.DeviceIdType.MESH)
+    pl.semaphore_wait(barrier, len(peers))
+
+    def window(c, bits, start=0, count=rows):
+        a, j = chunks[c]
+        at = pl.multiple_of((t ^ bits) * cols, 128)
+        return outs[a].at[j, pl.ds(start, count), pl.ds(at, cols)]
+
+    def copy(c, kind, src, dst, device):
+        return pltpu.make_async_remote_copy(
+            src_ref=src,
+            dst_ref=dst,
+            send_sem=send_sem.at[c, kind],
+            recv_sem=recv_sem.at[c, kind],
+            device_id=device,
+            device_id_type=pl.DeviceIdType.MESH,
+        )
+
+    started = []
+
+    def start(*args):
+        made = copy(*args)
+        made.start()
+        started.append(made)
+
+    def arrived(c, kind, dst, device):
+        copy(c, kind, dst, dst, device).wait_recv()
+
+    locals_ = []
+    for c, (a, j) in enumerate(chunks):
+        if far:
+            start(c, 0, sends[a].at[j], window(c, 0), {"sp": lax.rem(s + j + 1, n)})
+        else:
+            made = pltpu.make_async_copy(sends[a].at[j], window(c, 0), local_sem.at[c])
+            made.start()
+            locals_.append(made)
+    total = len(chunks)
+    for k in range(total + 2):
+        if k < total:
+            if far:
+                arrived(k, 0, window(k, 0), {"sp": lax.rem(s + 1, n)})
+                own = window(k, 0)
+            else:
+                own = sends[chunks[k][0]].at[chunks[k][1]]
+            start(k, 1, own, window(k, 0), across)
+            start(k, 2, own, window(k, 0), along)
+            start(k, 5, own, window(k, 0), other)
+        c = k - 1
+        if 0 <= c < total:
+            arrived(c, 1, window(c, 2), across)
+            start(c, 3, window(c, 2, 0, half), window(c, 2, 0, half), along)
+            start(c, 6, window(c, 2), window(c, 2), other)
+            arrived(c, 2, window(c, 4), along)
+            start(c, 4, window(c, 4, half, rows - half), window(c, 4, half, rows - half), across)
+            start(c, 7, window(c, 4), window(c, 4), other)
+        c = k - 2
+        if 0 <= c < total:
+            arrived(c, 3, window(c, 6, 0, half), along)
+            arrived(c, 4, window(c, 6, half, rows - half), across)
+            start(c, 8, window(c, 6), window(c, 6), other)
+    for c in range(total):
+        for kind, bits in ((5, 1), (6, 3), (7, 5), (8, 7)):
+            arrived(c, kind, window(c, bits), other)
+    for made in started:
+        made.wait_send()
+    for made in locals_:
+        made.wait()
+
+
+def spread(arrays, far, collective_id):
+    n = lax.axis_size("sp")
+    ranks = lax.axis_size("tp")
+    blocks, rows, cols = arrays[0].shape
+    count = len(arrays)
+    total = count * blocks
+    space = pl.ANY if far else pltpu.VMEM
+    got = pl.pallas_call(
+        functools.partial(spread_kernel, n, count, far),
+        out_shape=[jax.ShapeDtypeStruct((blocks, rows, ranks * cols), BF16)] * count,
+        in_specs=[pl.BlockSpec(memory_space=space)] * count,
+        out_specs=[pl.BlockSpec(memory_space=pl.ANY)] * count,
+        scratch_shapes=[
+            pltpu.SemaphoreType.DMA((total, 9)),
+            pltpu.SemaphoreType.DMA((total, 9)),
+            pltpu.SemaphoreType.DMA((total,)),
+        ],
+        compiler_params=pltpu.CompilerParams(collective_id=collective_id, has_side_effects=True),
+    )(*arrays)
+    return [g.reshape(blocks * rows, ranks * cols) for g in got]
 
 
 def body(
@@ -60,10 +170,7 @@
     away_weight = row_weight[1:].reshape((n - 1) * cap, 1)
     send_rows = dot(away, mixed_part).astype(BF16).reshape(n - 1, cap, share)
     send_scaled = (dot(away, cot_part) * away_weight).astype(BF16).reshape(n - 1, cap, share)
-    got_rows = jnp.concatenate([shift(send_rows[j - 1], j) for j in range(1, n)], axis=0)
-    got_scaled = jnp.concatenate([shift(send_scaled[j - 1], j) for j in range(1, n)], axis=0)
-    rem_rows = lax.all_gather(got_rows, "tp", axis=1, tiled=True)
-    rem_scaled = lax.all_gather(got_scaled, "tp", axis=1, tiled=True)
+    rem_rows, rem_scaled = spread([send_rows, send_scaled], True, 1)
     loc_rows = dot(onehot[0], mixed).astype(BF16)
     loc_scaled = (dot(onehot[0], cotangent) * row_weight[0][:, None]).astype(BF16)
 
@@ -161,11 +268,26 @@
     came = jnp.concatenate(came, axis=0)
     back = dot(onehot.reshape(n * cap, tok), came, 0, 0)
     grad_part = (cot_part.astype(F32) + back).astype(BF16)
-    grad_mixed = lax.all_gather(grad_part, "tp", axis=1, tiled=True)
+    (grad_mixed,) = spread([grad_part.reshape(2, tok // 2, share)], False, 2)
 
     out_grad = dot(grad_mixed, out_proj)
-    proj_part = dot(grad_mixed, gated_b, 0, 0).astype(BF16)
-    proj_grad = lax.psum_scatter(proj_part, "sp", scatter_dimension=0, tiled=True).astype(F32)
+    quarter = width // n
+    piece = quarter // lax.axis_size("tp")
+    lane = lax.axis_index("tp") * piece
+    if piece % 128 == 0:
+        send_mixed = jnp.stack(
+            [
+                lax.dynamic_slice_in_dim(grad_mixed, lax.rem(own + j, n) * quarter + lane, piece, 1)
+                for j in range(1, n)
+            ]
+        )
+        (far_mixed,) = spread([send_mixed], True, 3)
+        own_mixed = lax.dynamic_slice_in_dim(grad_mixed, own * quarter, quarter, 1)
+        far_gated = jnp.concatenate([shift(gated_b, j) for j in range(1, n)], axis=0)
+        proj_grad = dot(own_mixed, gated_b, 0, 0) + dot(far_mixed, far_gated, 0, 0)
+    else:
+        proj_part = dot(grad_mixed, gated_b, 0, 0).astype(BF16)
+        proj_grad = lax.psum_scatter(proj_part, "sp", scatter_dimension=0, tiled=True).astype(F32)
 
     outer = out_grad * silu
     outer_b = outer.astype(BF16)

time: 303 us -> 258 us (0.85)
  waiting for transfers between devices: 170 us -> 44.7 us
  Pallas kernels: 0 us -> 96.2 us
  starting transfers between devices: 36.9 us -> 25.7 us
  other arithmetic: 12.4 us -> 7.49 us
    pallas_call x0 -> x3, Pallas kernels: none -> 96.2 us  [spread(): pl.pallas_call(functools.partial(spread_kernel, n, count, far), out_shape...]
    all_gather x3 -> x0, waiting for transfers between devices: 53.6 us -> none  [the longest x1 34 us: body(): rem_scaled = lax.all_gather(got_scaled, 'tp', axis=1, tiled=True)]
    reduce_scatter x1 -> x0, waiting for transfers between devices: 24.1 us -> none  [body(): lax.psum_scatter(proj_part, 'sp', scatter_dimension=0, tiled=True)]
    ppermute x17 -> x14, waiting for transfers between devices: 38.5 us -> 14.6 us  [shift(): return lax.ppermute(x, 'sp', [(i, (i + by) % n) for i in range(n)])]
    reduce_scatter x1, waiting for transfers between devices: 53.8 us -> 30.1 us  [body(): summed = lax.psum_scatter(portion, 'tp', scatter_dimension=1, tiled=True)]
    ppermute x17 -> x14, starting transfers between devices: 36.7 us -> 25.7 us  [shift(): return lax.ppermute(x, 'sp', [(i, (i + by) % n) for i in range(n)])]
    unnamed x86 -> x90, local copies, waits for them, and re-layouts: 7.65 us -> 5.62 us
    dot_general x43 -> x44, matrix products: 58 us -> 58.2 us  [dot(): lax.dot_general(a, b, (((ca,), (cb,)), ((), ())), preferred_element_type=...]
  transfers between devices with their start and end apart: 22 -> 15, of which waited for: 13 -> 3; matrix products, arithmetic and copies ran while one was open for 18% -> 13% of each run, Pallas kernels for 0% -> 8%
where the time goes in v2:
time: 258 us; the launch traced here: 257 us
  Pallas kernels  96.2 us (37%)
  matrix products  58.2 us (23%)
  waiting for transfers between devices  44.7 us (17%)
  starting transfers between devices  25.7 us (10%)
  between operations  14.9 us (6%)
  local copies, waits for them, and re-layouts  9.88 us (4%)
  other arithmetic  7.49 us (3%)
    pallas_call x3, Pallas kernels, spread(): pl.pallas_call(functools.partial(spread_kernel, n, count, far), out_shape...  96.2 us
    dot_general x44, matrix products, dot(): lax.dot_general(a, b, (((ca,), (cb,)), ((), ())), preferred_element_type=...  58.2 us
    reduce_scatter x1, waiting for transfers between devices, body(): summed = lax.psum_scatter(portion, 'tp', scatter_dimension=1, tiled=True)  30.1 us
    ppermute x14, starting transfers between devices, shift(): return lax.ppermute(x, 'sp', [(i, (i + by) % n) for i in range(n)])  25.7 us
    ppermute x14, waiting for transfers between devices, shift(): return lax.ppermute(x, 'sp', [(i, (i + by) % n) for i in range(n)])  14.6 us
    unnamed x90, local copies, waits for them, and re-layouts  5.62 us
  transfers between devices with their start and end apart: 15, of which 3 were waited for; matrix products, arithmetic and copies ran while one was open for 13% of the time, Pallas kernels for 8%

profile of v2, /device:TPU:0, one launch (start us, length us, event | category | flops | bytes accessed | tf_op | source)
XLA Modules:
  0.0 257.1 jit_solution(7609990974686661867)
XLA Ops:
  7.2 0.8 compare_select_fusion
  8.2 0.7 select_reduce_fusion.1
  9.5 3.3 %convolution_convert_fusion = bf16[192,4096]{1,0:T(8,128)(2,1)} fusion(bf16[256,4096]{1,0:T(8,128)(2,1)} %param.19, pred[4,192,256]{2,1,0:T(32,128)(4,1)S(1)} %iota_compare_fusion), kind=kOutput, calls=%fused_computation.9 | convolution fusion | flops 403439616 | bytes 3719168 | tf_op jit(solution)/shard_map/dot_general | solution.py:18
  12.9 2.1 convolution_convert_fusion.1
  15.0 2.1 fusion.22
  17.1 59.9 %shard_map.188 = (bf16[3,192,4096]{2,1,0:T(8,128)(2,1)}, bf16[3,192,4096]{2,1,0:T(8,128)(2,1)}) custom-call(bf16[3,192,512]{2,1,0:T(8,128)(2,1)} %bitcast.143, bf16[3,192,512]{2,1,0:T(8,128)(2,1)} %bitcast.144), custom_call_target="tpu_custom_call" | custom-call | tf_op jit(solution)/shard_map/pallas_call | solution.py:117
  76.9 4.5 %fusion.14 = f32[576,256]{1,0:T(8,128)S(1)} fusion(bf16[576,4096]{1,0:T(8,128)(2,1)} %bitcast.155, bf16[1,4096,256]{2,1,0:T(8,128)(2,1)} %param.24), kind=kOutput, calls=%fused_computation.20 | convolution fusion | flops 1207959552 | bytes 7405568 | tf_op jit(solution)/shard_map/dot_general | solution.py:18
  81.5 1.4 fusion.9
  83.0 0.6 fusion.11
  83.6 0.6 fusion.16
  84.3 1.2 copy-done.7
  85.6 0.6 fusion.3
  86.2 0.5 copy-done.9
  86.7 1.4 fusion.18
  88.1 0.8 fusion.20
  89.0 1.2 multiply_convert_fusion
  90.2 1.8 fusion.7
  92.0 5.7 %add_convert_fusion = bf16[768,4096]{1,0:T(8,128)(2,1)} fusion(f32[768,4096]{1,0:T(8,128)S(1)} %fusion.7, bf16[768,256]{1,0:T(8,128)(2,1)} %get-tuple-element.45, bf16[1,4096,256]{2,1,0:T(8,128)(2,1)S(1)} %copy-done.6), kind=kOutput, calls=%fused_computation | convolution fusion | flops 1616904192 | bytes 21364736 | tf_op jit(solution)/shard_map/dot_general | solution.py:18
  97.8 0.7 copy-done.32
  98.5 1.2 reduce-window.6
  100.7 6.3 %collective-permute-start.8 = (bf16[260,128]{1,0:T(8,128)(2,1)S(1)}, bf16[260,128]{1,0:T(8,128)(2,1)S(1)}, u32[]{:S(2)}, u32[]{:S(2)}) collective-permute-start(bf16[260,128]{1,0:T(8,128)(2,1)S(1)} %pad_maximum_fusion.4), channel_id=1, source_target_pairs={{0,8},{8,16},{16,24},{24,0},{1,9},{9,17},{17,25},{25,1},{2,10},{10... | collective-permute-start | bytes 199688 | tf_op jit(solution)/shard_map/ppermute | solution.py:23
  107.1 1.9 collective-permute-start.9
  109.0 0.5 collective-permute-start.10
  109.5 1.9 collective-permute-start.4
  111.5 1.0 collective-permute-start.6
  112.8 0.9 fusion.73
  113.7 0.9 fusion.76
  114.6 0.9 fusion.79
  115.5 0.9 fusion.82
  116.4 4.5 %fusion.51 = f32[256,4096]{1,0:T(8,128)S(1)} fusion(bf16[576,4096]{1,0:T(8,128)(2,1)} %bitcast.139, bf16[768,256]{1,0:T(8,128)(2,1)S(1)} %get-tuple-element.43), kind=kOutput, calls=%fused_computation.87 | convolution fusion | flops 1207959552 | bytes 9207808 | tf_op jit(solution)/shard_map/dot_general | solution.py:18
  121.0 2.1 fusion.4
  123.1 1.9 fusion.53
  125.0 2.1 fusion.5
  127.1 1.9 fusion.55
  129.0 2.1 fusion.6
  131.3 0.9 bitcast_compare_fusion
  132.6 0.7 mul.197
  133.8 30.1 %reduce-scatter.2.cloned.1.call-done = bf16[768,512]{1,0:T(8,128)(2,1)} async-done(((bf16[768,4096]{1,0:T(8,128)(2,1)}), bf16[768,512]{1,0:T(8,128)(2,1)}) %reduce-scatter.2.cloned.1.call-update) | async-done | bytes 786448 | tf_op jit(solution)/shard_map/reduce_scatter | solution.py:258
  163.9 1.3 fusion.108
  165.2 3.4 %collective-permute-start = (bf16[192,512]{1,0:T(8,128)(2,1)S(1)}, bf16[192,512]{1,0:T(8,128)(2,1)S(1)}, u32[]{:S(2)}, u32[]{:S(2)}) collective-permute-start(bf16[192,512]{1,0:T(8,128)(2,1)S(1)} %get-tuple-element.49), channel_id=1, source_target_pairs={{0,24},{8,0},{16,8},{24,16},{1,25},{9,1},{17,9},{25,17},{2,26},{10... | collective-permute-start | bytes 589832 | tf_op jit(solution)/shard_map/ppermute | solution.py:23
  168.6 1.1 collective-permute-start.2
  169.7 1.0 fusion.69
  170.7 3.2 %collective-permute-done = bf16[192,512]{1,0:T(8,128)(2,1)S(1)} collective-permute-done((bf16[192,512]{1,0:T(8,128)(2,1)S(1)}, bf16[192,512]{1,0:T(8,128)(2,1)S(1)}, u32[]{:S(2)}, u32[]{:S(2)}) %collective-permute-start) | collective-permute-done | bytes 196640 | tf_op jit(solution)/shard_map/ppermute | solution.py:23
  173.9 11.4 %collective-permute-done.1 = bf16[192,512]{1,0:T(8,128)(2,1)S(1)} collective-permute-done((bf16[192,512]{1,0:T(8,128)(2,1)S(1)}, bf16[192,512]{1,0:T(8,128)(2,1)S(1)}, u32[]{:S(2)}, u32[]{:S(2)}) %collective-permute-start.1) | collective-permute-done | bytes 196640 | tf_op jit(solution)/shard_map/ppermute | solution.py:23
  185.3 2.3 fusion.23
  187.6 15.0 %shard_map.189 = bf16[2,128,4096]{2,1,0:T(8,128)(2,1)} custom-call(bf16[2,128,512]{2,1,0:T(8,128)(2,1)} %bitcast.149), custom_call_target="tpu_custom_call" | custom-call | tf_op jit(solution)/shard_map/pallas_call | solution.py:117
  202.7 2.6 %fusion.110 = f32[256,256]{0,1:T(8,128)S(1)} fusion(bf16[256,4096]{1,0:T(8,128)(2,1)} %bitcast.136, bf16[4096,256]{1,0:T(8,128)(2,1)S(1)} %copy-done.8), kind=kOutput, calls=%fused_computation.186 | convolution fusion | flops 536870912 | bytes 4456448 | tf_op jit(solution)/shard_map/dot_general | solution.py:18
  205.4 0.3 multiply_convert_fusion.3
  205.7 1.1 collective-permute-start.11
  206.8 2.0 collective-permute-start.12
  210.4 2.9 %collective-permute-start.3 = (bf16[256,128]{1,0:T(8,128)(2,1)S(1)}, bf16[256,128]{1,0:T(8,128)(2,1)S(1)}, u32[]{:S(2)}, u32[]{:S(2)}) collective-permute-start(bf16[256,128]{1,0:T(8,128)(2,1)S(1)} %convolution_convert_fusion.3), channel_id=1, source_target_pairs={{0,24},{8,0},{16,8},{24,16},{1,25},{9,1},{17,9},{25,17},{2,26},{10... | collective-permute-start | bytes 196616 | tf_op jit(solution)/shard_map/ppermute | solution.py:23
  213.4 0.5 collective-permute-start.7
  214.9 1.4 fusion.44
  216.3 0.9 fusion.34
  217.1 0.9 dynamic-slice_bitcast_fusion.2
  218.1 0.7 pad_maximum_fusion.3.refs_0_
  218.8 21.3 %shard_map.190 = bf16[3,256,1024]{2,1,0:T(8,128)(2,1)} custom-call(bf16[3,256,128]{2,1,0:T(8,128)(2,1)} %pad_maximum_fusion.3.refs_0_), custom_call_target="tpu_custom_call" | custom-call | tf_op jit(solution)/shard_map/pallas_call | solution.py:117
  240.1 0.8 copy.45
  240.9 2.8 %collective-permute-start.13 = (bf16[256,256]{0,1:T(8,128)(2,1)S(1)}, bf16[256,256]{0,1:T(8,128)(2,1)}, u32[]{:S(2)}, u32[]{:S(2)}) collective-permute-start(bf16[256,256]{0,1:T(8,128)(2,1)S(1)} %get-tuple-element.50), channel_id=1, source_target_pairs={{0,24},{8,0},{16,8},{24,16},{1,25},{9,1},{17,9},{25,17},{2,26},{10... | collective-permute-start | bytes 393224 | tf_op jit(solution)/shard_map/ppermute | solution.py:23
  244.0 0.8 copy.44
  244.8 0.9 fusion.33
  245.7 0.6 copy-done.18
  246.4 0.6 copy-done.19
  247.0 3.2 %convolution_add_fusion.3 = f32[1024,256]{1,0:T(8,128)} fusion(f32[1024,256]{1,0:T(8,128)S(1)} %fusion.44, bf16[768,1024]{1,0:T(8,128)(2,1)} %bitcast.135, bf16[256,256]{0,1:T(8,128)(2,1)} %collective-permute-done.13, bf16[256,256]{0,1:T(8,128)(2,1)} %copy-done.19, bf16[256,256]{0,1:T(8,128)(2,1)} %copy-done.18), kind=kOutput, calls=%fused_computation.29 | convolution fusion | flops 404094976 | bytes 4063232 | tf_op jit(solution)/shard_map/dot_general | solution.py:18
  (154 shorter events, 6.4 us)
Async XLA Ops:
  7.2 74.3 %copy-start = (bf16[1,4096,256]{2,1,0:T(8,128)(2,1)S(1)}, bf16[1,4096,256]{2,1,0:T(8,128)(2,1)}, u32[]{:S(2)}) copy-start(bf16[1,4096,256]{2,1,0:T(8,128)(2,1)} %param.23) | copy-start | bytes 6291460
  7.2 156.7 %reduce-scatter.2.cloned.1.call-start = ((), (), s32[]{:S(2)}) async-start(), calls=%async_computation.1 | async-start | bytes 7077888 | tf_op jit(solution)/shard_map/reduce_scatter | solution.py:258
  8.2 0.8 copy-start.24
  9.3 5.6 %copy-start.26 = (f32[4,192]{1,0:T(4,128)}, f32[4,192]{1,0:T(4,128)S(1)}, u32[]{:S(2)}) copy-start(f32[4,192]{1,0:T(4,128)S(1)} %select_reduce_fusion) | copy-start | bytes 9220
  76.9 4.6 %copy-start.37 = (bf16[3,192,4096]{2,1,0:T(8,128)(2,1)S(1)}, bf16[3,192,4096]{2,1,0:T(8,128)(2,1)}, u32[]{:S(2)}) copy-start(bf16[3,192,4096]{2,1,0:T(8,128)(2,1)} %get-tuple-element.11) | copy-start | bytes 14155780
  81.5 1.4 copy-start.2
  81.5 2.1 copy-start.6
  82.9 3.3 %slice-start = ((s8[4718592]{0:T(1024)(128)(4,1)}), s8[4194304]{0:T(1024)(128)(4,1)S(1)}, s32[]{:S(2)}) async-start(s8[4718592]{0:T(1024)(128)(4,1)} %bitcast.140), calls=%async_computation.2 | async-start | bytes 8388608
  83.6 1.9 copy-start.7
  83.6 2.0 slice-start.2
  83.6 2.6 %slice-start.1 = ((s8[4718592]{0:T(1024)(128)(4,1)}), s8[524288]{0:T(1024)(128)(4,1)S(1)}, s32[]{:S(2)}) async-start(s8[4718592]{0:T(1024)(128)(4,1)} %bitcast.140), calls=%async_computation.3 | async-start | bytes 1048576
  84.3 2.4 copy-start.9
  86.2 1.9 copy-start.4
  97.8 0.7 copy-start.32
  97.8 2.5 copy-start.13
  97.8 2.7 %copy-start.12 = (bf16[256,128]{1,0:T(8,128)(2,1)S(1)}, bf16[256,128]{1,0:T(8,128)(2,1)}, u32[]{:S(2)}) copy-start(bf16[256,128]{1,0:T(8,128)(2,1)} %param.14) | copy-start | bytes 196612
  97.8 14.8 %copy-start.11 = (bf16[256,128]{1,0:T(8,128)(2,1)S(1)}, bf16[256,128]{1,0:T(8,128)(2,1)}, u32[]{:S(2)}) copy-start(bf16[256,128]{1,0:T(8,128)(2,1)} %param.15) | copy-start | bytes 196612
  100.7 32.6 %collective-permute-start.8 = (bf16[260,128]{1,0:T(8,128)(2,1)S(1)}, bf16[260,128]{1,0:T(8,128)(2,1)S(1)}, u32[]{:S(2)}, u32[]{:S(2)}) collective-permute-start(bf16[260,128]{1,0:T(8,128)(2,1)S(1)} %pad_maximum_fusion.4), channel_id=1, source_target_pairs={{0,8},{8,16},{16,24},{24,0},{1,9},{9,17},{17,25},{25,1},{2,10},{10... | collective-permute-start | bytes 199688 | tf_op jit(solution)/shard_map/ppermute | solution.py:23
  107.1 26.3 %collective-permute-start.9 = (bf16[260,128]{1,0:T(8,128)(2,1)S(1)}, bf16[260,128]{1,0:T(8,128)(2,1)S(1)}, u32[]{:S(2)}, u32[]{:S(2)}) collective-permute-start(bf16[260,128]{1,0:T(8,128)(2,1)S(1)} %pad_maximum_fusion.4), channel_id=1, source_target_pairs={{0,16},{8,24},{16,0},{24,8},{1,17},{9,25},{17,1},{25,9},{2,18},{10... | collective-permute-start | bytes 199688 | tf_op jit(solution)/shard_map/ppermute | solution.py:23
  109.0 60.7 %collective-permute-start.10 = (bf16[260,128]{1,0:T(8,128)(2,1)S(1)}, bf16[260,128]{1,0:T(8,128)(2,1)}, u32[]{:S(2)}, u32[]{:S(2)}) collective-permute-start(bf16[260,128]{1,0:T(8,128)(2,1)S(1)} %pad_maximum_fusion.4), channel_id=1, source_target_pairs={{0,24},{8,0},{16,8},{24,16},{1,25},{9,1},{17,9},{25,17},{2,26},{10... | collective-permute-start | bytes 199688 | tf_op jit(solution)/shard_map/ppermute | solution.py:23
  109.5 22.7 %collective-permute-start.4 = (bf16[4,128]{1,0:T(4,128)(2,1)S(1)}, bf16[4,128]{1,0:T(4,128)(2,1)S(1)}, u32[]{:S(2)}, u32[]{:S(2)}) collective-permute-start(bf16[4,128]{1,0:T(4,128)(2,1)S(1)} %broadcast_in_dim.99), channel_id=1, source_target_pairs={{0,24},{8,0},{16,8},{24,16},{1,25},{9,1},{17,9},{25,17},{2,26},{10... | collective-permute-start | bytes 3080 | tf_op jit(solution)/shard_map/ppermute | solution.py:23
  111.5 20.8 %collective-permute-start.6 = (bf16[4,128]{1,0:T(4,128)(2,1)S(1)}, bf16[4,128]{1,0:T(4,128)(2,1)S(1)}, u32[]{:S(2)}, u32[]{:S(2)}) collective-permute-start(bf16[4,128]{1,0:T(4,128)(2,1)S(1)} %broadcast_in_dim.99), channel_id=1, source_target_pairs={{0,16},{8,24},{16,0},{24,8},{1,17},{9,25},{17,1},{25,9},{2,18},{10... | collective-permute-start | bytes 3080 | tf_op jit(solution)/shard_map/ppermute | solution.py:23
  112.5 8.4 %copy-start.28 = (f32[256]{0:T(256)}, f32[256]{0:T(256)S(1)}, u32[]{:S(2)}) copy-start(f32[256]{0:T(256)S(1)} %get-tuple-element.56) | copy-start | bytes 3076
  112.5 8.4 %copy-start.30 = (f32[256]{0:T(256)}, f32[256]{0:T(256)S(1)}, u32[]{:S(2)}) copy-start(f32[256]{0:T(256)S(1)} %get-tuple-element.57) | copy-start | bytes 3076
  112.5 8.4 %copy-start.33 = (f32[256]{0:T(256)}, f32[256]{0:T(256)S(1)}, u32[]{:S(2)}) copy-start(f32[256]{0:T(256)S(1)} %get-tuple-element.55) | copy-start | bytes 3076
  112.5 8.4 %copy-start.35 = (f32[256]{0:T(256)}, f32[256]{0:T(256)S(1)}, u32[]{:S(2)}) copy-start(f32[256]{0:T(256)S(1)} %get-tuple-element.54) | copy-start | bytes 3076
  112.7 3.6 %copy-start.15 = (f32[256,256]{1,0:T(8,128)}, f32[256,256]{1,0:T(8,128)S(1)}, u32[]{:S(2)}) copy-start(f32[256,256]{1,0:T(8,128)S(1)} %fusion.109) | copy-start | bytes 786436
  113.7 9.4 %slice-start.3 = ((s8[4718592]{0:T(1024)(128)(4,1)}), s8[4194304]{0:T(1024)(128)(4,1)S(1)}, s32[]{:S(2)}) async-start(s8[4718592]{0:T(1024)(128)(4,1)} %bitcast.157), calls=%async_computation.5 | async-start | bytes 8388608
  116.4 4.6 %copy-start.5 = (bf16[192,4096]{1,0:T(8,128)(2,1)S(1)}, bf16[192,4096]{1,0:T(8,128)(2,1)}, u32[]{:S(2)}) copy-start(bf16[192,4096]{1,0:T(8,128)(2,1)} %copy-done.4) | copy-start | bytes 4718596
  116.4 6.7 %slice-start.4 = ((s8[4718592]{0:T(1024)(128)(4,1)}), s8[524288]{0:T(1024)(128)(4,1)S(1)}, s32[]{:S(2)}) async-start(s8[4718592]{0:T(1024)(128)(4,1)} %bitcast.157), calls=%async_computation.6 | async-start | bytes 1048576
  121.0 2.1 copy-start.10
  123.1 1.9 copy-start.3
  129.0 2.3 copy-start.25
  129.0 3.1 %copy-start.17 = (bf16[256,256]{1,0:T(8,128)(2,1)S(1)}, bf16[256,256]{1,0:T(8,128)(2,1)}, u32[]{:S(2)}) copy-start(bf16[256,256]{1,0:T(8,128)(2,1)} %param.17) | copy-start | bytes 393220
  165.2 8.7 %collective-permute-start = (bf16[192,512]{1,0:T(8,128)(2,1)S(1)}, bf16[192,512]{1,0:T(8,128)(2,1)S(1)}, u32[]{:S(2)}, u32[]{:S(2)}) collective-permute-start(bf16[192,512]{1,0:T(8,128)(2,1)S(1)} %get-tuple-element.49), channel_id=1, source_target_pairs={{0,24},{8,0},{16,8},{24,16},{1,25},{9,1},{17,9},{25,17},{2,26},{10... | collective-permute-start | bytes 589832 | tf_op jit(solution)/shard_map/ppermute | solution.py:23
  168.6 16.7 %collective-permute-start.1 = (bf16[192,512]{1,0:T(8,128)(2,1)S(1)}, bf16[192,512]{1,0:T(8,128)(2,1)S(1)}, u32[]{:S(2)}, u32[]{:S(2)}) collective-permute-start(bf16[192,512]{1,0:T(8,128)(2,1)S(1)} %get-tuple-element.48), channel_id=1, source_target_pairs={{0,16},{8,24},{16,0},{24,8},{1,17},{9,25},{17,1},{25,9},{2,18},{10... | collective-permute-start | bytes 589832 | tf_op jit(solution)/shard_map/ppermute | solution.py:23
  168.6 16.7 %collective-permute-start.2 = (bf16[192,512]{1,0:T(8,128)(2,1)S(1)}, bf16[192,512]{1,0:T(8,128)(2,1)S(1)}, u32[]{:S(2)}, u32[]{:S(2)}) collective-permute-start(bf16[192,512]{1,0:T(8,128)(2,1)S(1)} %get-tuple-element.47), channel_id=1, source_target_pairs={{0,8},{8,16},{16,24},{24,0},{1,9},{9,17},{17,25},{25,1},{2,10},{10... | collective-permute-start | bytes 589832 | tf_op jit(solution)/shard_map/ppermute | solution.py:23
  185.3 17.3 %copy-start.8 = (bf16[4096,256]{1,0:T(8,128)(2,1)S(1)}, bf16[4096,256]{1,0:T(8,128)(2,1)}, u32[]{:S(2)}) copy-start(bf16[4096,256]{1,0:T(8,128)(2,1)} %param.18) | copy-start | bytes 6291460
  202.6 2.7 %copy-start.20 = (f32[256,64]{0,1:T(8,128)S(1)}, f32[256,64]{0,1:T(8,128)}, u32[]{:S(2)}) copy-start(f32[256,64]{0,1:T(8,128)} %fusion.73) | copy-start | bytes 196612
  202.6 2.7 %copy-start.21 = (f32[256,64]{0,1:T(8,128)S(1)}, f32[256,64]{0,1:T(8,128)}, u32[]{:S(2)}) copy-start(f32[256,64]{0,1:T(8,128)} %fusion.76) | copy-start | bytes 196612
  202.6 2.7 %copy-start.22 = (f32[256,64]{0,1:T(8,128)S(1)}, f32[256,64]{0,1:T(8,128)}, u32[]{:S(2)}) copy-start(f32[256,64]{0,1:T(8,128)} %fusion.79) | copy-start | bytes 196612
  202.6 2.7 %copy-start.23 = (f32[256,64]{0,1:T(8,128)S(1)}, f32[256,64]{0,1:T(8,128)}, u32[]{:S(2)}) copy-start(f32[256,64]{0,1:T(8,128)} %fusion.82) | copy-start | bytes 196612
  202.6 6.1 %copy-start.14 = (bf16[256,256]{1,0:T(8,128)(2,1)S(1)}, bf16[256,256]{1,0:T(8,128)(2,1)}, u32[]{:S(2)}) copy-start(bf16[256,256]{1,0:T(8,128)(2,1)} %param.13) | copy-start | bytes 393220
  202.7 6.1 %copy-start.36 = (f32[256]{0:T(256)S(1)}, f32[256]{0:T(256)}, u32[]{:S(2)}) copy-start(f32[256]{0:T(256)} %copy-done.35) | copy-start | bytes 3076
  205.3 3.7 %copy-start.31 = (f32[256]{0:T(256)S(1)}, f32[256]{0:T(256)}, u32[]{:S(2)}) copy-start(f32[256]{0:T(256)} %copy-done.30) | copy-start | bytes 3076
  205.3 4.0 %copy-start.29 = (f32[256]{0:T(256)S(1)}, f32[256]{0:T(256)}, u32[]{:S(2)}) copy-start(f32[256]{0:T(256)} %copy-done.28) | copy-start | bytes 3076
  205.3 4.2 %copy-start.34 = (f32[256]{0:T(256)S(1)}, f32[256]{0:T(256)}, u32[]{:S(2)}) copy-start(f32[256]{0:T(256)} %copy-done.33) | copy-start | bytes 3076
  205.4 8.5 %copy-start.16 = (f32[256,256]{1,0:T(8,128)S(1)}, f32[256,256]{1,0:T(8,128)}, u32[]{:S(2)}) copy-start(f32[256,256]{1,0:T(8,128)} %copy-done.15) | copy-start | bytes 786436
  205.7 40.0 %collective-permute-start.11 = (bf16[256,256]{0,1:T(8,128)(2,1)S(1)}, bf16[256,256]{0,1:T(8,128)(2,1)S(1)}, u32[]{:S(2)}, u32[]{:S(2)}) collective-permute-start(bf16[256,256]{0,1:T(8,128)(2,1)S(1)} %get-tuple-element.50), channel_id=1, source_target_pairs={{0,8},{8,16},{16,24},{24,0},{1,9},{9,17},{17,25},{25,1},{2,10},{10... | collective-permute-start | bytes 393224 | tf_op jit(solution)/shard_map/ppermute | solution.py:23
  206.8 38.9 %collective-permute-start.12 = (bf16[256,256]{0,1:T(8,128)(2,1)S(1)}, bf16[256,256]{0,1:T(8,128)(2,1)S(1)}, u32[]{:S(2)}, u32[]{:S(2)}) collective-permute-start(bf16[256,256]{0,1:T(8,128)(2,1)S(1)} %get-tuple-element.50), channel_id=1, source_target_pairs={{0,16},{8,24},{16,0},{24,8},{1,17},{9,25},{17,1},{25,9},{2,18},{10... | collective-permute-start | bytes 393224 | tf_op jit(solution)/shard_map/ppermute | solution.py:23
  210.4 30.5 %collective-permute-start.3 = (bf16[256,128]{1,0:T(8,128)(2,1)S(1)}, bf16[256,128]{1,0:T(8,128)(2,1)S(1)}, u32[]{:S(2)}, u32[]{:S(2)}) collective-permute-start(bf16[256,128]{1,0:T(8,128)(2,1)S(1)} %convolution_convert_fusion.3), channel_id=1, source_target_pairs={{0,24},{8,0},{16,8},{24,16},{1,25},{9,1},{17,9},{25,17},{2,26},{10... | collective-permute-start | bytes 196616 | tf_op jit(solution)/shard_map/ppermute | solution.py:23
  213.3 30.4 %collective-permute-start.5 = (bf16[256,128]{1,0:T(8,128)(2,1)S(1)}, bf16[256,128]{1,0:T(8,128)(2,1)S(1)}, u32[]{:S(2)}, u32[]{:S(2)}) collective-permute-start(bf16[256,128]{1,0:T(8,128)(2,1)S(1)} %convolution_convert_fusion.3), channel_id=1, source_target_pairs={{0,16},{8,24},{16,0},{24,8},{1,17},{9,25},{17,1},{25,9},{2,18},{10... | collective-permute-start | bytes 196616 | tf_op jit(solution)/shard_map/ppermute | solution.py:23
  213.4 30.3 %collective-permute-start.7 = (bf16[256,128]{1,0:T(8,128)(2,1)S(1)}, bf16[256,128]{1,0:T(8,128)(2,1)S(1)}, u32[]{:S(2)}, u32[]{:S(2)}) collective-permute-start(bf16[256,128]{1,0:T(8,128)(2,1)S(1)} %convolution_convert_fusion.3), channel_id=1, source_target_pairs={{0,8},{8,16},{16,24},{24,0},{1,9},{9,17},{17,25},{25,1},{2,10},{10... | collective-permute-start | bytes 196616 | tf_op jit(solution)/shard_map/ppermute | solution.py:23
  216.3 27.4 %copy-start.27 = (f32[256]{0:T(256)S(1)}, f32[256]{0:T(256)}, u32[]{:S(2)}) copy-start(f32[256]{0:T(256)} %mul.197) | copy-start | bytes 3076
  240.9 6.1 %collective-permute-start.13 = (bf16[256,256]{0,1:T(8,128)(2,1)S(1)}, bf16[256,256]{0,1:T(8,128)(2,1)}, u32[]{:S(2)}, u32[]{:S(2)}) collective-permute-start(bf16[256,256]{0,1:T(8,128)(2,1)S(1)} %get-tuple-element.50), channel_id=1, source_target_pairs={{0,24},{8,0},{16,8},{24,16},{1,25},{9,1},{17,9},{25,17},{2,26},{10... | collective-permute-start | bytes 393224 | tf_op jit(solution)/shard_map/ppermute | solution.py:23
  245.7 0.6 copy-start.18
  246.4 0.6 copy-start.19
  247.0 3.2 %copy-start.1 = (bf16[1,4096,256]{2,1,0:T(8,128)(2,1)S(1)}, bf16[1,4096,256]{2,1,0:T(8,128)(2,1)}, u32[]{:S(2)}) copy-start(bf16[1,4096,256]{2,1,0:T(8,128)(2,1)} %param.23) | copy-start | bytes 6291460
Sparse Core Ops, SparseCore 0:
  97.9 65.9 reduce-scatter.1
